TPU v7x, 32 devices: a whole 2x2x4 slice. The times are simulated.
32 devices in a mesh: sp: 16 (over z, y, core), tp: 2 (over x).
Axes of the slice: x: 2, y: 2, z: 4, core: 2. Of those that a mesh axis runs over, the one named last changes fastest.
Arguments:
- tokens: bfloat16 [8192, 2048], P(('sp', 'tp')), may hold values from -6 to 6
- norm_gain: float32 [2048], replicated, may hold values from 0.1 to 1.9
- query_weight: bfloat16 [2048, 1024], P(None, 'tp'), may hold values from -0.13258252 to 0.13258252
- key_weight: bfloat16 [2048, 1024], P(None, 'tp'), may hold values from -0.13258252 to 0.13258252
- value_weight: bfloat16 [2048, 1024], P(None, 'tp'), may hold values from -0.125 to 0.125
- glu_value_weight: bfloat16 [2048, 1024], P(None, 'tp'), may hold values from -0.125 to 0.125
- glu_gate_weight: bfloat16 [2048, 1024], P(None, 'tp'), may hold values from -0.125 to 0.125
- qk_gain: float32 [2, 64], replicated, may hold values from 1 to 6
- mix_lambda: float32 [8], P('tp'), may hold values from 0.3 to 0.8
- head_gain: float32 [128], replicated, may hold values from 0.1 to 1.9
- conv_kernel: float32 [31, 1024], P(None, 'tp'), may hold values from -1 to 1
- channel_gain: float32 [1024], P('tp'), may hold values from 0.1 to 1.9
- channel_shift: float32 [1024], P('tp'), may hold values from -3 to 3
- output_weight: bfloat16 [2048, 2048], replicated, may hold values from -0.125 to 0.125
Outputs:
- mixed: bfloat16 [8192, 2048], P(('sp', 'tp'))
- log_totals: float32 [2, 8, 8192], P(None, 'tp', 'sp')
All inputs are finite; a program needn't handle non-finite values.
Results may differ from a plain program's by a relative error of at most 0.035.
Values may be sent and summed in bfloat16 or wider, within the bound.
A program may use at most 128 MiB of HBM per device.

v0:
```python
import math

import jax
import jax.numpy as jnp
from jax import lax
from jax.experimental import pallas as pl
from jax.experimental.pallas import tpu as pltpu
from jax.sharding import PartitionSpec as P

MESH = pl.DeviceIdType.MESH
NEG = -1e30


def from_behind(value, axis, steps):
    count = lax.axis_size(axis)
    leading, last = (max(0, -steps), min(count, count - steps))
    return lax.ppermute(value, axis, [(source, source + steps) for source in range(leading, last)])


def flipped(g, a, group):
    if group % 2:
        return g
    return jnp.where(a % 2 == 0, g, group - 1 - g)


def spread_kernel(ways, group, q_ref, kv_ref, qo_ref, kvo_ref, qsend, qrecv, ksend, kfwd, krelay, krecv, local):
    me = lax.axis_index("sp")
    a = me // group
    g = me % group
    cores = 2 if group % 2 == 0 else 1
    half = group // cores
    mate = a * group + (g + 1 - 2 * (g % 2)) if cores == 2 else me

    def same(d):
        return (g + d * cores) % group

    peers = [lax.rem(a + d, ways) * group + g for d in range(1, ways)]
    peers += [a * group + same(d) for d in range(1, half)]
    if cores == 2:
        peers.append(mate)
        peers += [lax.rem(a + d, ways) * group + group - 1 - g for d in range(ways)]
    barrier = pltpu.get_barrier_semaphore()
    for peer in peers:
        pl.semaphore_signal(barrier, inc=1, device_id={"sp": peer}, device_id_type=MESH)
    pl.semaphore_wait(barrier, len(peers))

    def kv_copy(src, slot, send, peer):
        return pltpu.make_async_remote_copy(
            src_ref=src, dst_ref=kvo_ref.at[slot], send_sem=send, recv_sem=krecv.at[slot],
            device_id={"sp": peer}, device_id_type=MESH)

    sends = []
    keep = pltpu.make_async_copy(kv_ref.at[a], kvo_ref.at[me], local.at[0])
    keep_q = pltpu.make_async_copy(q_ref.at[a], qo_ref.at[a], local.at[1])
    keep.start()

    def q_copy(h, slot, d):
        return pltpu.make_async_remote_copy(
            src_ref=q_ref.at[h], dst_ref=qo_ref.at[slot], send_sem=qsend.at[d], recv_sem=qrecv.at[slot],
            device_id={"sp": h * group + flipped(g, a, group)}, device_id_type=MESH)

    stays = a % 2 == 0 if cores == 2 else a >= 0

    @pl.when(stays)
    def _():
        keep_q.start()
    order = list(range(1, ways))
    for d in order:
        h = lax.rem(a + d, ways)
        c = kv_copy(kv_ref.at[h], me, ksend.at[d - 1], h * group + g)
        c.start()
        sends.append(c)

    def forward(d):
        src_a = lax.rem(a + ways - d, ways)
        slot = src_a * group + g
        if d:
            kv_copy(kvo_ref.at[slot], slot, ksend.at[d - 1], me).wait_recv()
            src = kvo_ref.at[slot]
        else:
            src = kv_ref.at[a]
        n = 0
        for e in range(1, half):
            c = kv_copy(src, slot, kfwd.at[d, n], a * group + same(e))
            c.start()
            sends.append(c)
            n += 1
        if cores == 2:
            c = kv_copy(src, slot, kfwd.at[d, n], mate)
            c.start()
            sends.append(c)

    def relay(d):
        src_a = lax.rem(a + ways - d, ways)
        for e in range(1, half):
            slot = src_a * group + same(e)
            kv_copy(kvo_ref.at[slot], slot, krelay.at[d, e - 1], mate).wait_recv()
            if cores == 2:
                c = kv_copy(kvo_ref.at[slot], slot, krelay.at[d, e - 1], mate)
                c.start()
                sends.append(c)

    forward(0)
    for d in order:
        c = q_copy(lax.rem(a + d, ways), a, d)
        c.start()
        sends.append(c)
    if cores == 2:
        @pl.when(jnp.logical_not(stays))
        def _():
            q_copy(a, a, 0).start()
    for d in range(1, ways):
        forward(d)
        relay(d - 1)
    relay(ways - 1)
    if cores == 2:
        for d in range(ways):
            src_a = lax.rem(a + ways - d, ways)
            for e in range(half):
                slot = src_a * group + (g + 1 - 2 * (g % 2) + e * cores) % group
                kv_copy(kvo_ref.at[slot], slot, krelay.at[0, 0], mate).wait_recv()
    for d in range(1, ways):
        src_a = lax.rem(a + ways - d, ways)
        q_copy(a, src_a, d).wait_recv()
    for c in sends:
        c.wait_send()
    keep.wait()

    @pl.when(stays)
    def _():
        keep_q.wait()

    if cores == 2:
        @pl.when(jnp.logical_not(stays))
        def _():
            q_copy(a, a, 0).wait()


def spread(q, kv, ways, group):
    cores = 2 if group % 2 == 0 else 1
    half = group // cores
    any_ = pl.BlockSpec(memory_space=pl.ANY)
    n = max(ways - 1, 1)
    return pl.pallas_call(
        lambda *refs: spread_kernel(ways, group, *refs),
        out_shape=(
            jax.ShapeDtypeStruct(q.shape, q.dtype),
            jax.ShapeDtypeStruct((ways * group,) + kv.shape[1:], kv.dtype),
        ),
        in_specs=[any_, any_],
        out_specs=(any_, any_),
        scratch_shapes=[
            pltpu.SemaphoreType.DMA((ways,)),
            pltpu.SemaphoreType.DMA((ways,)),
            pltpu.SemaphoreType.DMA((n,)),
            pltpu.SemaphoreType.DMA((ways, half)),
            pltpu.SemaphoreType.DMA((ways, max(half - 1, 1))),
            pltpu.SemaphoreType.DMA((ways * group,)),
            pltpu.SemaphoreType.DMA((2,)),
        ],
        compiler_params=pltpu.CompilerParams(collective_id=1, has_side_effects=True),
        name="spread",
    )(q, kv)


def collect_kernel(ways, group, tp, att_ref, lt_ref, conv_ref, ao_ref, lo_ref, co_ref, asend, arecv, lsend, lrecv, csend, crecv, local):
    me = lax.axis_index("sp")
    t = lax.axis_index("tp")
    a = me // group
    g = me % group
    vdim = att_ref.shape[-1]
    cch = conv_ref.shape[-1]

    def coords(i):
        dt, da = i % tp, i // tp
        return lax.rem(a + da, ways), lax.rem(t + dt, tp)

    total = ways * tp
    both = group % 2 == 0
    barrier = pltpu.get_barrier_semaphore()
    for i in range(total):
        pa, pt = coords(i)
        if i:
            pl.semaphore_signal(barrier, inc=1, device_id={"sp": pa * group + g, "tp": pt}, device_id_type=MESH)
        if both:
            pl.semaphore_signal(
                barrier, inc=1, device_id={"sp": pa * group + group - 1 - g, "tp": pt}, device_id_type=MESH)
    pl.semaphore_wait(barrier, 2 * total - 1 if both else total - 1)

    head = t * ways + a

    def att_copy(i, slot):
        pa, pt = coords(i)
        return pltpu.make_async_remote_copy(
            src_ref=att_ref.at[pa, pt], dst_ref=ao_ref.at[slot], send_sem=asend.at[i], recv_sem=arecv.at[slot],
            device_id={"sp": pa * group + flipped(g, pa, group), "tp": pt}, device_id_type=MESH)

    def lt_copy(i, slot):
        pa = lax.rem(a + i, ways)
        return pltpu.make_async_remote_copy(
            src_ref=lt_ref.at[pa], dst_ref=lo_ref.at[slot], send_sem=lsend.at[i], recv_sem=lrecv.at[slot],
            device_id={"sp": pa * group + flipped(g, pa, group), "tp": t}, device_id_type=MESH)

    stays = a % 2 == 0 if both else a >= 0
    sends = []
    for i in range(total - 1, 0, -1):
        c = att_copy(i, head)
        c.start()
        sends.append(c)
    for i in range(1, tp):
        pa, pt = coords(i)
        c = pltpu.make_async_remote_copy(
            src_ref=conv_ref.at[pt], dst_ref=co_ref.at[t],
            send_sem=csend.at[i], recv_sem=crecv.at[t],
            device_id={"sp": me, "tp": pt}, device_id_type=MESH)
        c.start()
        sends.append(c)
    for i in range(1, ways):
        c = lt_copy(i, a)
        c.start()
        sends.append(c)
    keep = pltpu.make_async_copy(conv_ref.at[t], co_ref.at[t], local.at[1])
    keep.start()
    mine = [
        pltpu.make_async_copy(att_ref.at[a, t], ao_ref.at[head], local.at[0]),
        pltpu.make_async_copy(lt_ref.at[a], lo_ref.at[a], local.at[2]),
    ]

    @pl.when(stays)
    def _():
        for c in mine:
            c.start()

    if both:
        @pl.when(jnp.logical_not(stays))
        def _():
            att_copy(0, head).start()
            lt_copy(0, a).start()
    for i in range(1, total):
        pa, pt = coords(i)
        att_copy(i, pt * ways + pa).wait_recv()
    for i in range(1, tp):
        pa, pt = coords(i)
        pltpu.make_async_remote_copy(
            src_ref=conv_ref.at[t], dst_ref=co_ref.at[pt],
            send_sem=csend.at[i], recv_sem=crecv.at[pt],
            device_id={"sp": me, "tp": pt}, device_id_type=MESH).wait_recv()
    for i in range(1, ways):
        lt_copy(i, lax.rem(a + i, ways)).wait_recv()
    for c in sends:
        c.wait_send()
    keep.wait()

    @pl.when(stays)
    def _():
        for c in mine:
            c.wait()

    if both:
        @pl.when(jnp.logical_not(stays))
        def _():
            att_copy(0, head).wait()
            lt_copy(0, a).wait()


def collect(att, lt, conv, ways, group, tp):
    any_ = pl.BlockSpec(memory_space=pl.ANY)
    rows, vdim = att.shape[2:]
    total = ways * tp
    return pl.pallas_call(
        lambda *refs: collect_kernel(ways, group, tp, *refs),
        out_shape=(
            jax.ShapeDtypeStruct((total, rows, vdim), att.dtype),
            jax.ShapeDtypeStruct(lt.shape, lt.dtype),
            jax.ShapeDtypeStruct(conv.shape, conv.dtype),
        ),
        in_specs=[any_] * 3,
        out_specs=(any_,) * 3,
        scratch_shapes=[
            pltpu.SemaphoreType.DMA((total,)),
            pltpu.SemaphoreType.DMA((total,)),
            pltpu.SemaphoreType.DMA((ways,)),
            pltpu.SemaphoreType.DMA((ways,)),
            pltpu.SemaphoreType.DMA((tp,)),
            pltpu.SemaphoreType.DMA((tp,)),
            pltpu.SemaphoreType.DMA((3,)),
        ],
        compiler_params=pltpu.CompilerParams(collective_id=2, has_side_effects=True),
        name="collect",
    )(att, lt, conv)


def attention(place, lam, head_gain, qt, kv, tile=512):
    ways, qdim, rows = qt.shape
    hd = qdim // 2
    blocks = kv.shape[0]
    vdim = head_gain.shape[0]
    group = blocks // ways
    tile = math.gcd(tile, rows)
    tiles = rows // tile
    def kernel(place_ref, lam_ref, gain_ref, q_ref, kv_ref, o_ref, lt_ref, sa, sb, acc_ref):
        i = pl.program_id(0); s = pl.program_id(1)
        chunk = i * group + flipped(place_ref[0], i, group)
        qs = [q_ref[0, m * hd:(m + 1) * hd, :] for m in range(2)]
        def score(j, ref):
            for m in range(2):
                ref[m] = jnp.dot(kv_ref[j, :rows, m * hd:(m + 1) * hd], qs[m], preferred_element_type=jnp.float32)
        def absorb(j, ref, tops, masked=False):
            vb = jnp.concatenate([kv_ref[j, rows + b * vdim:rows + (b + 1) * vdim] for b in range(rows // 128)], axis=1)
            vb = jnp.concatenate([vb, jnp.ones((16, rows), jnp.bfloat16)], axis=0)
            out=[]
            for m in range(2):
                sc = ref[m]
                if masked:
                    kp = lax.broadcasted_iota(jnp.int32, sc.shape, 0)
                    qp = lax.broadcasted_iota(jnp.int32, sc.shape, 1) + s * tile
                    sc = jnp.where(kp <= qp, sc, NEG)
                new = jnp.maximum(tops[m], jnp.max(sc, axis=0, keepdims=True))
                p = jnp.exp(sc - new)
                f = jnp.exp(tops[m] - new)
                acc_ref[m] = acc_ref[m] * f + jnp.dot(vb, p.astype(jnp.bfloat16), preferred_element_type=jnp.float32)
                out.append(new)
            return tuple(out)
        acc_ref[...] = jnp.zeros_like(acc_ref)
        one = jnp.full((1, tile), NEG, jnp.float32)
        score(chunk, sa)
        score(0, sb)
        tops = absorb(chunk, sa, (one, one), True)

        def pair(j, tops):
            score(2 * j + 1, sa)
            tops = absorb(2 * j, sb, tops)
            score(2 * j + 2, sb)
            return absorb(2 * j + 1, sa, tops)

        tops = lax.fori_loop(0, chunk // 2, pair, tops)
        tops = lax.cond(chunk % 2 == 1, lambda t: absorb(chunk - 1, sb, t), lambda t: t, tops)
        a0=acc_ref[0]; a1=acc_ref[1]
        t0,t1=tops
        l0=a0[vdim:vdim+1]; l1=a1[vdim:vdim+1]; a0=a0[:vdim]; a1=a1[:vdim]
        heads = a0 / l0 - lam_ref[0] * a1 / l1
        heads = heads * lax.rsqrt(jnp.mean(heads * heads, axis=0, keepdims=True) + 1e-06) * gain_ref[...]
        o_ref[0] = heads.T.astype(jnp.bfloat16)
        lt_ref[0, 0:1, :] = t0 + jnp.log(l0)
        lt_ref[0, 1:2, :] = t1 + jnp.log(l1)
    smem = pl.BlockSpec(memory_space=pltpu.SMEM)
    return pl.pallas_call(kernel, grid=(ways, tiles),
        out_shape=(jax.ShapeDtypeStruct((ways, rows, vdim), jnp.bfloat16), jax.ShapeDtypeStruct((ways, 2, rows), jnp.float32)),
        in_specs=[smem, smem, pl.BlockSpec((vdim, 1), lambda i, s: (0, 0)), pl.BlockSpec((1, qdim, tile), lambda i, s: (i, 0, s)), pl.BlockSpec(kv.shape, lambda i, s: (0, 0, 0))],
        out_specs=(pl.BlockSpec((1, tile, vdim), lambda i, s: (i, s, 0)), pl.BlockSpec((1, 2, tile), lambda i, s: (i, 0, s))),
        scratch_shapes=[pltpu.VMEM((2,rows,tile),jnp.float32),pltpu.VMEM((2,rows,tile),jnp.float32),pltpu.VMEM((2,vdim+16,tile),jnp.float32)],
        compiler_params=pltpu.CompilerParams(vmem_limit_bytes=58 << 20), name="attend")(place, lam, head_gain.reshape(-1, 1), qt, kv)


def prepare_t(raw, qk_gain, cosine, sine):
    values = raw.astype(jnp.float32)
    values = values * lax.rsqrt(jnp.mean(values * values, axis=2, keepdims=True) + 1e-06)
    values = values * qk_gain[None, :, :, None]
    half = raw.shape[2] // 2
    first, second = values[:, :, :half], values[:, :, half:]
    return jnp.concatenate(
        [first * cosine - second * sine, second * cosine + first * sine], axis=2
    ).astype(jnp.bfloat16)


def per_device(
    tokens, norm_gain, query_weight, key_weight, value_weight, glu_value_weight, glu_gate_weight,
    qk_gain, mix_lambda, head_gain, conv_kernel, channel_gain, channel_shift, output_weight,
):
    head_size = qk_gain.shape[1]
    heads_here = mix_lambda.shape[0]
    value_size = head_gain.shape[0]
    kernel_len = conv_kernel.shape[0]
    conv_here = conv_kernel.shape[1]
    width = tokens.shape[1]
    sp = lax.axis_size("sp")
    tp = lax.axis_size("tp")
    me = lax.axis_index("sp")
    t = lax.axis_index("tp")
    ways = heads_here
    group = sp // ways
    own = tokens.shape[0]
    rows = own * tp

    def norm(piece):
        inputs = piece.astype(jnp.float32)
        return (
            inputs * lax.rsqrt(jnp.mean(inputs * inputs, axis=-1, keepdims=True) + 1e-06) * norm_gain
        ).astype(jnp.bfloat16)

    others = [tokens] + [
        lax.ppermute(tokens, "tp", [(i, (i - d) % tp) for i in range(tp)]) for d in range(1, tp)
    ]
    if tp == 2:
        other = others[1]
        normed = norm(jnp.concatenate([jnp.where(t == 0, tokens, other), jnp.where(t == 0, other, tokens)], axis=0))
    else:
        stacked = jnp.stack(others)
        normed = norm(jnp.concatenate(
            [lax.dynamic_index_in_dim(stacked, (j - t) % tp, 0, keepdims=False) for j in range(tp)], axis=0))

    def turned(matrix):
        return lax.dot_general(matrix, normed, (((0,), (1,)), ((), ())), preferred_element_type=jnp.float32).astype(jnp.bfloat16)

    def plain(matrix):
        return jnp.dot(normed, matrix, preferred_element_type=jnp.float32).astype(jnp.bfloat16)

    positions = (me * rows + jnp.arange(rows, dtype=jnp.int32)).astype(jnp.float32)
    inverse = 10000.0 ** (-jnp.arange(0, head_size // 2, dtype=jnp.float32) * 2.0 / head_size)
    angles = positions[None, :] * inverse[:, None]
    cosine, sine = jnp.cos(angles)[None, None], jnp.sin(angles)[None, None]
    shape = (heads_here, 2, head_size, rows)
    rq = prepare_t(turned(query_weight).reshape(shape), qk_gain, cosine, sine) * jnp.bfloat16(head_size ** -0.5)
    rk = prepare_t(turned(key_weight).reshape(shape), qk_gain, cosine, sine)
    qt = rq.reshape(heads_here, 2 * head_size, rows)
    kk = jnp.transpose(rk.reshape(heads_here, 2 * head_size, rows), (0, 2, 1))
    vt = turned(value_weight).reshape(heads_here, value_size, rows)
    kv = jnp.concatenate([kk, vt.reshape(heads_here, value_size, rows // 128, 128).transpose(0, 2, 1, 3).reshape(heads_here, -1, 128)], axis=1)
    qall, kvall = spread(qt, kv, ways, group)

    glu_a, glu_g = plain(glu_value_weight), plain(glu_gate_weight)
    gated = (glu_a.astype(jnp.float32) * jax.nn.sigmoid(glu_g.astype(jnp.float32))).astype(jnp.bfloat16)
    earlier = from_behind(gated[rows - (kernel_len - 1):], "sp", 1)
    extended = jnp.concatenate([earlier, gated], axis=0).astype(jnp.float32)
    convolved = jnp.zeros((rows, conv_here), jnp.float32)
    for step in range(kernel_len):
        convolved = convolved + conv_kernel[step][None, :] * extended[step:step + rows]
    plain_sum, square_sum = lax.psum(
        (jnp.sum(convolved, axis=1), jnp.sum(convolved * convolved, axis=1)), "tp"
    )
    channels = conv_here * tp
    middle = (plain_sum / channels)[:, None]
    spread_ = (square_sum / channels)[:, None] - middle * middle
    conv_out = jax.nn.silu(
        (convolved - middle) * lax.rsqrt(spread_ + 1e-05) * channel_gain + channel_shift
    ).astype(jnp.bfloat16)

    place = (me % group).astype(jnp.int32).reshape(1)
    lam = lax.dynamic_slice(mix_lambda, (me // group,), (1,))
    att, lt = attention(place, lam, head_gain, qall, kvall)
    ao, lo, co = collect(
        att.reshape(ways, tp, own, value_size), lt, conv_out.reshape(tp, own, conv_here), ways, group, tp)
    heads = ways * tp
    merged = jnp.concatenate([
        jnp.transpose(ao, (1, 0, 2)).reshape(own, heads * value_size),
        jnp.transpose(co, (1, 0, 2)).reshape(own, channels)], axis=1)
    mixed = jnp.dot(merged, output_weight, preferred_element_type=jnp.float32).astype(jnp.bfloat16)
    return (mixed, jnp.transpose(lo, (1, 0, 2)))


def solution(mesh):
    placed = (
        P(("sp", "tp"), None), P(), P(None, "tp"), P(None, "tp"), P(None, "tp"), P(None, "tp"), P(None, "tp"),
        P(), P("tp"), P(), P(None, "tp"), P("tp"), P("tp"), P(),
    )
    return jax.shard_map(
        per_device,
        mesh=mesh,
        in_specs=placed,
        out_specs=(P(("sp", "tp"), None), P(None, "tp", "sp")),
        check_vma=False,
    )
```

profile of v0, /device:TPU:11, one launch (start us, length us, event | category | flops | bytes accessed | tf_op | source)
XLA Modules:
  0.0 171.5 jit_solution(7921875561589893534)
XLA Ops:
  1.0 1.5 copy.24.gain_ref
  2.5 1.3 dynamic_slice.3.lam_ref
  3.8 1.0 fusion.56
  4.8 1.8 %fusion.55 = (f32[1,512]{1,0:T(1,128)S(1)}, f32[1,512]{1,0:T(1,128)S(1)}, f32[1,512]{1,0:T(1,128)S(1)}, f32[1,512]{1,0:T(1,128)S(1)}, f32[1,512]{1,0:T(1,128)S(1...) fusion(f32[31,512]{1,0:T(8,128)} %param.24), kind=kLoop, calls=%fused_computation.114 | loop fusion | bytes 77824 | tf_op jit(solution)/shard_map/slice | solution.py:427
  6.9 18.2 %collective-permute-done = bf16[256,2048]{1,0:T(8,128)(2,1)} collective-permute-done((bf16[256,2048]{1,0:T(8,128)(2,1)}, bf16[256,2048]{1,0:T(8,128)(2,1)}, u32[]{:S(2)}, u32[]{:S(2)}) %collective-permute-start) | collective-permute-done | bytes 1048608 | tf_op jit(solution)/shard_map/ppermute | solution.py:392
  25.1 1.7 broadcast_select_fusion.1
  26.8 0.5 fusion
  27.3 1.5 copy-done.22
  28.7 1.5 fusion.7
  30.3 1.3 fusion.12
  31.7 0.8 copy-done.4
  32.4 4.9 %collective-permute-start.1 = (bf16[30,512]{1,0:T(8,128)(2,1)S(1)}, bf16[30,512]{1,0:T(8,128)(2,1)S(1)}, u32[]{:S(2)}, u32[]{:S(2)}) collective-permute-start(bf16[30,512]{1,0:T(8,128)(2,1)S(1)} %slice.272), channel_id=1, source_target_pairs={{0,2},{2,4},{4,6},{6,8},{8,10},{10,12},{12,14},{14,16},{16,18},{18... | collective-permute-start | bytes 92168 | tf_op jit(solution)/shard_map/ppermute | solution.py:17
  37.3 1.4 multiply_reduce_fusion.2
  38.8 1.5 multiply_reduce_fusion.1
  40.8 1.1 subtract_convert_fusion
  41.9 0.8 pad_maximum_fusion.2
  42.7 2.0 %copy.22 = bf16[4,128,512]{1,2,0:T(8,128)(2,1)} copy(bf16[4,128,512]{2,1,0:T(8,128)(2,1)} %bitcast.68) | data formatting | bytes 1048576 | tf_op jit(solution)/shard_map/convert_element_type | solution.py:363
  44.7 4.0 %fusion.13 = bf16[512,512]{0,1:T(8,128)(2,1)} fusion(bf16[2048,512]{1,0:T(8,128)(2,1)} %param.18, f32[2048]{0:T(1024)} %param.15, f32[512]{0:T(512)} %copy-done.20, bf16[256,2048]{1,0:T(8,128)(2,1)} %copy-done.1, bf16[256,2048]{1,0:T(8,128)(2,1)S(1)} %get-tuple-element.25), kind=kOutput, calls=%fused_computation.22 | convolution fusion | flops 1081344000 | bytes 4728832 | tf_op jit(solution)/shard_map/dot_general | solution.py:403
  48.8 1.2 reshape_reshape.3
  50.0 1.1 copy.23
  51.1 2.1 %pad_maximum_fusion.1.refs_1_ = bf16[4,1024,128]{2,1,0:T(8,128)(2,1)} fusion(bf16[4,512,128]{2,1,0:T(8,128)(2,1)} %bitcast.70, bf16[4,512,128]{2,1,0:T(8,128)(2,1)S(1)} %bitcast.69), kind=kLoop, calls=%fused_computation.84 | loop fusion | flops 2097152 | bytes 2097152 | tf_op jit(solution)/shard_map/concatenate | solution.py:418
  53.3 0.9 maximum_multiply_fusion
  54.2 40.7 %spread.1 = (bf16[4,128,512]{2,1,0:T(8,128)(2,1)}, bf16[16,1024,128]{2,1,0:T(8,128)(2,1)}) custom-call(bf16[4,128,512]{2,1,0:T(8,128)(2,1)} %bitcast.67, bf16[4,1024,128]{2,1,0:T(8,128)(2,1)} %pad_maximum_fusion.1.refs_1_), custom_call_target="tpu_custom_call" | custom-call | tf_op jit(solution)/shard_map/spread/pallas_call | solution.py:144
  95.0 26.6 %attend.1 = (bf16[4,512,128]{2,1,0:T(8,128)(2,1)}, f32[4,2,512]{2,1,0:T(2,128)}) custom-call(s32[1]{0:T(128)} %bitcast.place_ref, f32[1]{0:T(128)} %dynamic_slice.3.lam_ref, f32[128,1]{1,0:T(8,128)} %copy.24.gain_ref, bf16[4,128,512]{2,1,0:T(8,128)(2,1)} %get-tuple-element.9.q_ref, bf16[16,1024,128]{2,1,0:T(8,128)(2,1)} %get-tuple-element.10.kv_ref), custom_call_target="tpu_custom_call" | custom-call | tf_op jit(solution)/shard_map/attend/pallas_call | solution.py:347
  121.9 5.1 %fusion.53 = (f32[512]{0:T(512)S(1)}, f32[512]{0:T(512)S(1)}, f32[512,512]{1,0:T(8,128)S(1)}) fusion(f32[542,512]{1,0:T(8,128)S(1)} %maximum_convert_fusion, f32[512]{0:T(512)S(1)} %bitcast.87, f32[512]{0:T(512)S(1)} %bitcast.88, f32[512]{0:T(512)S(1)} %bitcast.90, f32[512]{0:T(512)S(1)} %bitcast.91, f32[512]{0:T(512)S(1)} %bitcast.92, f32[512]{0:T(512)S(1)} %bitcast.93, ...), kind=kLoop, calls=%fused_computation.113 | loop fusion | flops 16776192 | bytes 33622016 | tf_op jit(solution)/shard_map/reduce_sum | solution.py:429
  127.0 4.0 %all-reduce = (f32[512]{0:T(512)S(1)}, f32[512]{0:T(512)S(1)}) all-reduce(f32[512]{0:T(512)S(1)} %get-tuple-element.21, f32[512]{0:T(512)S(1)} %get-tuple-element.20), channel_id=1, replica_groups=mesh['sp'=16,'tp'=2] {'tp'}, use_global_device_ids=true, to_apply=%region_6.7 | all-reduce | flops 1024 | bytes 8192 | tf_op jit(solution)/shard_map/psum | solution.py:428
  131.0 1.2 multiply_convert_fusion
  132.2 29.4 %collect.1 = (bf16[8,256,128]{2,1,0:T(8,128)(2,1)}, f32[4,2,512]{2,1,0:T(2,128)}, bf16[2,256,512]{2,1,0:T(8,128)(2,1)}) custom-call(bf16[4,2,256,128]{3,2,1,0:T(8,128)(2,1)} %bitcast.71, f32[4,2,512]{2,1,0:T(2,128)} %get-tuple-element.12.refs_1_, bf16[2,256,512]{2,1,0:T(8,128)(2,1)} %bitcast.66), custom_call_target="tpu_custom_call" | custom-call | tf_op jit(solution)/shard_map/collect/pallas_call | solution.py:270
  161.7 1.3 copy.25
  162.9 1.2 copy.26
  164.2 0.6 copy.27
  164.8 6.7 %convolution_convert_fusion = bf16[256,2048]{1,0:T(8,128)(2,1)} fusion(bf16[2048,2048]{1,0:T(8,128)(2,1)} %param.27, bf16[256,1024]{0,1:T(8,128)(2,1)S(1)} %bitcast.75, bf16[256,1024]{0,1:T(8,128)(2,1)S(1)} %bitcast.74), kind=kOutput, calls=%fused_computation.5 | convolution fusion | flops 2150105088 | bytes 10485760 | tf_op jit(solution)/shard_map/dot_general | solution.py:447
  (61 shorter events, 1.6 us)
Async XLA Ops:
  0.6 36.7 %copy-start = (bf16[2048,512]{1,0:T(8,128)(2,1)S(1)}, bf16[2048,512]{1,0:T(8,128)(2,1)}, u32[]{:S(2)}) copy-start(bf16[2048,512]{1,0:T(8,128)(2,1)} %param.16) | copy-start | bytes 6291460
  0.6 24.4 %collective-permute-start = (bf16[256,2048]{1,0:T(8,128)(2,1)}, bf16[256,2048]{1,0:T(8,128)(2,1)}, u32[]{:S(2)}, u32[]{:S(2)}) collective-permute-start(bf16[256,2048]{1,0:T(8,128)(2,1)} %param.14), channel_id=1, source_target_pairs={{0,1},{1,0},{2,3},{3,2},{4,5},{5,4},{6,7},{7,6},{8,9},{9,8},{10,11... | collective-permute-start | bytes 3145736 | tf_op jit(solution)/shard_map/ppermute | solution.py:392
  26.8 12.0 %copy-start.1 = (bf16[256,2048]{1,0:T(8,128)(2,1)}, bf16[256,2048]{1,0:T(8,128)(2,1)S(1)}, u32[]{:S(2)}) copy-start(bf16[256,2048]{1,0:T(8,128)(2,1)S(1)} %get-tuple-element.26) | copy-start | bytes 3145732
  26.8 2.0 %copy-start.22 = (bf16[2048,512]{1,0:T(8,128)(2,1)S(1)}, bf16[2048,512]{1,0:T(8,128)(2,1)}, u32[]{:S(2)}) copy-start(bf16[2048,512]{1,0:T(8,128)(2,1)} %param.20) | copy-start | bytes 6291460
  26.8 2.0 %copy-start.25 = (f32[2048]{0:T(1024)S(1)}, f32[2048]{0:T(1024)}, u32[]{:S(2)}) copy-start(f32[2048]{0:T(1024)} %param.15) | copy-start | bytes 24580
  28.7 10.0 %copy-start.20 = (f32[512]{0:T(512)}, f32[512]{0:T(512)S(1)}, u32[]{:S(2)}) copy-start(f32[512]{0:T(512)S(1)} %add_rsqrt_fusion.3) | copy-start | bytes 6148
  28.7 1.6 copy-start.23
  31.6 0.8 copy-start.4
  32.4 6.3 %copy-start.24 = (bf16[2048,512]{1,0:T(8,128)(2,1)S(1)}, bf16[2048,512]{1,0:T(8,128)(2,1)}, u32[]{:S(2)}) copy-start(bf16[2048,512]{1,0:T(8,128)(2,1)} %param.17) | copy-start | bytes 6291460
  32.4 89.2 %collective-permute-start.1 = (bf16[30,512]{1,0:T(8,128)(2,1)S(1)}, bf16[30,512]{1,0:T(8,128)(2,1)S(1)}, u32[]{:S(2)}, u32[]{:S(2)}) collective-permute-start(bf16[30,512]{1,0:T(8,128)(2,1)S(1)} %slice.272), channel_id=1, source_target_pairs={{0,2},{2,4},{4,6},{6,8},{8,10},{10,12},{12,14},{14,16},{16,18},{18... | collective-permute-start | bytes 92168 | tf_op jit(solution)/shard_map/ppermute | solution.py:17
  38.8 1.5 copy-start.21
  48.8 2.4 %copy-start.2 = (bf16[4,128,512]{1,2,0:T(8,128)(2,1)S(1)}, bf16[4,128,512]{1,2,0:T(8,128)(2,1)}, u32[]{:S(2)}) copy-start(bf16[4,128,512]{1,2,0:T(8,128)(2,1)} %copy.22) | copy-start | bytes 1572868
  51.1 2.1 %copy-start.3 = (bf16[4,2,32,512]{3,2,1,0:T(8,128)(2,1)S(1)}, bf16[4,2,32,512]{3,2,1,0:T(8,128)(2,1)}, u32[]{:S(2)}) copy-start(bf16[4,2,32,512]{3,2,1,0:T(8,128)(2,1)} %get-tuple-element.32) | copy-start | bytes 786436
  94.9 26.7 %copy-start.5 = (bf16[512,512]{1,0:T(8,128)(2,1)S(1)}, bf16[512,512]{1,0:T(8,128)(2,1)}, u32[]{:S(2)}) copy-start(bf16[512,512]{1,0:T(8,128)(2,1)} %copy-done.4) | copy-start | bytes 1572868
  94.9 26.9 %copy-start.7 = (f32[1,512]{1,0:T(1,128)S(1)}, f32[1,512]{1,0:T(1,128)}, u32[]{:S(2)}) copy-start(f32[1,512]{1,0:T(1,128)} %get-tuple-element.41) | copy-start | bytes 6148
  94.9 26.9 %copy-start.8 = (f32[1,512]{1,0:T(1,128)S(1)}, f32[1,512]{1,0:T(1,128)}, u32[]{:S(2)}) copy-start(f32[1,512]{1,0:T(1,128)} %get-tuple-element.42) | copy-start | bytes 6148
  94.9 26.9 %copy-start.9 = (f32[1,512]{1,0:T(1,128)S(1)}, f32[1,512]{1,0:T(1,128)}, u32[]{:S(2)}) copy-start(f32[1,512]{1,0:T(1,128)} %get-tuple-element.43) | copy-start | bytes 6148
  94.9 26.9 %copy-start.10 = (f32[1,512]{1,0:T(1,128)S(1)}, f32[1,512]{1,0:T(1,128)}, u32[]{:S(2)}) copy-start(f32[1,512]{1,0:T(1,128)} %get-tuple-element.44) | copy-start | bytes 6148
  94.9 26.9 %copy-start.11 = (f32[1,512]{1,0:T(1,128)S(1)}, f32[1,512]{1,0:T(1,128)}, u32[]{:S(2)}) copy-start(f32[1,512]{1,0:T(1,128)} %get-tuple-element.45) | copy-start | bytes 6148
  95.0 26.9 %copy-start.12 = (f32[1,512]{1,0:T(1,128)S(1)}, f32[1,512]{1,0:T(1,128)}, u32[]{:S(2)}) copy-start(f32[1,512]{1,0:T(1,128)} %get-tuple-element.46) | copy-start | bytes 6148
  95.0 26.9 %copy-start.13 = (f32[1,512]{1,0:T(1,128)S(1)}, f32[1,512]{1,0:T(1,128)}, u32[]{:S(2)}) copy-start(f32[1,512]{1,0:T(1,128)} %get-tuple-element.47) | copy-start | bytes 6148
  95.0 26.9 %copy-start.14 = (f32[1,512]{1,0:T(1,128)S(1)}, f32[1,512]{1,0:T(1,128)}, u32[]{:S(2)}) copy-start(f32[1,512]{1,0:T(1,128)} %get-tuple-element.48) | copy-start | bytes 6148
  95.0 26.9 %copy-start.15 = (f32[1,512]{1,0:T(1,128)S(1)}, f32[1,512]{1,0:T(1,128)}, u32[]{:S(2)}) copy-start(f32[1,512]{1,0:T(1,128)} %get-tuple-element.49) | copy-start | bytes 6148
  95.0 26.9 %copy-start.16 = (f32[1,512]{1,0:T(1,128)S(1)}, f32[1,512]{1,0:T(1,128)}, u32[]{:S(2)}) copy-start(f32[1,512]{1,0:T(1,128)} %get-tuple-element.50) | copy-start | bytes 6148
  95.0 26.9 %copy-start.17 = (f32[1,512]{1,0:T(1,128)S(1)}, f32[1,512]{1,0:T(1,128)}, u32[]{:S(2)}) copy-start(f32[1,512]{1,0:T(1,128)} %get-tuple-element.51) | copy-start | bytes 6148
  121.9 9.1 %copy-start.18 = (f32[512]{0:T(512)S(1)}, f32[512]{0:T(512)}, u32[]{:S(2)}) copy-start(f32[512]{0:T(512)} %param.26) | copy-start | bytes 6148
  121.9 9.1 %copy-start.19 = (f32[512]{0:T(512)S(1)}, f32[512]{0:T(512)}, u32[]{:S(2)}) copy-start(f32[512]{0:T(512)} %param.25) | copy-start | bytes 6148
  161.6 2.5 %copy-start.6 = (f32[4,2,512]{2,1,0:T(2,128)S(1)}, f32[4,2,512]{2,1,0:T(2,128)}, u32[]{:S(2)}) copy-start(f32[4,2,512]{2,1,0:T(2,128)} %get-tuple-element.15) | copy-start | bytes 49156
where the time goes:
time: 172 us; the launch traced here: 171 us
  Pallas kernels  96.7 us (56%)
  waiting for transfers between devices  18.2 us (11%)
  matrix products  16.4 us (10%)
  local copies, waits for them, and re-layouts  15.6 us (9%)
  other arithmetic  14.3 us (8%)
  starting transfers between devices  5.19 us (3%)
  blocking collectives  4.01 us (2%)
    pallas_call x1, Pallas kernels, spread(): pl.pallas_call(lambda *refs: spread_kernel(ways, group, *refs), out_shape...  40.7 us
    pallas_call x1, Pallas kernels, collect(): pl.pallas_call(lambda *refs: collect_kernel(ways, group, tp, *refs), out_...  29.4 us
    pallas_call x1, Pallas kernels, attention(): pl.pallas_call(kernel, grid=(ways, tiles), out_shape=(jax.ShapeDtypeStruc...  26.6 us
    ppermute x1, waiting for transfers between devices, per_device(): lax.ppermute(tokens, 'tp', [(i, (i - d) % tp) for i in range(tp)])  18.2 us
    dot_general x3, matrix products, turned(): lax.dot_general(matrix, normed, (((0,), (1,)), ((), ())), preferred_eleme...  6.93 us
    dot_general x1, matrix products, per_device(): jnp.dot(merged, output_weight, preferred_element_type=jnp.float32)  6.7 us
    reduce_sum x1, other arithmetic, per_device(): jnp.sum(convolved, axis=1)  5.05 us
    ppermute x1, starting transfers between devices, from_behind(): lax.ppermute(value, axis, [(source, source + steps) for source in range(l...  4.87 us
  transfers between devices with their start and end apart: 2, of which 1 were waited for; matrix products, arithmetic and copies ran while one was open for 13% of the time, Pallas kernels for 39%

commit v1 on v0

--- a/solution.py
+++ b/solution.py
@@ -362,6 +362,517 @@
         [first * cosine - second * sine, second * cosine + first * sine], axis=2
     ).astype(jnp.bfloat16)
 
+PIECES = 4
+
+
+def layer_kernel(
+    sizes, tokens_ref, gain_ref, wq_ref, wk_ref, wv_ref, wa_ref, wg_ref, tab_ref, lam_ref, hgain_ref, taps_ref,
+    cgain_ref, cshift_ref, wo_ref, mixed_ref, lo_ref,
+    toks, w, tab, wo, nrm, raw, qs, kvs, qbuf, kvbuf, gext, glast, halo, conv, cvo, cvr, st, str_, macc,
+    sa, sb, acc, aos, ao, lts, lor,
+    load, tok_send, tok_recv, q_send, q_recv, kv_send, kv_recv, y_send, m_send, halo_send, halo_recv,
+    st_send, st_recv, cv_send, cv_recv, ao_send, ao_recv, lt_send, lt_recv,
+):
+    ways, group, tp, taps = sizes
+    s = lax.axis_index("sp")
+    t = lax.axis_index("tp")
+    a = s // group
+    g = s % group
+    sp = ways * group
+    other = 1 - t
+    prow = nrm.shape[0]
+    rows = PIECES * prow
+    hd = qbuf.shape[2] // 2
+    vdim = hgain_ref.shape[1]
+    cch = conv.shape[2]
+    channels = cch * tp
+    half = hd // 2
+    mate = a * group + g + 1 - 2 * (g % 2)
+    across = a * group + (g + 2) % group
+    stays = a % 2 == 0
+
+    def turn(i):
+        return g + (i % 2) * (group - 1 - 2 * g)
+
+    def remote(src, dst, send, recv, row, col):
+        return pltpu.make_async_remote_copy(
+            src_ref=src, dst_ref=dst, send_sem=send, recv_sem=recv,
+            device_id={"sp": row, "tp": col}, device_id_type=MESH)
+
+    loads = [pltpu.make_async_copy(tokens_ref.at[pl.ds(j * prow, prow)], toks.at[j], load.at[j]) for j in range(2)]
+    loads += [
+        pltpu.make_async_copy(ref, w.at[n], load.at[2 + n]) for n, ref in enumerate((wq_ref, wk_ref, wv_ref, wa_ref, wg_ref))]
+    loads.append(pltpu.make_async_copy(tab_ref, tab, load.at[7]))
+    out_load = pltpu.make_async_copy(wo_ref, wo, load.at[8])
+    for c in loads:
+        c.start()
+    out_load.start()
+
+    barrier = pltpu.get_barrier_semaphore()
+    flat = s * tp + t
+
+    def greet(n, carry):
+        to = lax.rem(flat + n, sp * tp)
+        pl.semaphore_signal(barrier, inc=1, device_id={"sp": to // tp, "tp": to % tp}, device_id_type=MESH)
+        return carry
+
+    lax.fori_loop(1, sp * tp, greet, 0)
+    pl.semaphore_wait(barrier, sp * tp - 1)
+
+    def tok_copy(j):
+        return remote(
+            tokens_ref.at[pl.ds(j * prow, prow)], toks.at[2 + j], tok_send.at[j], tok_recv.at[j], s, other)
+
+    for j in range(2):
+        tok_copy(j).start()
+
+    def piece_of(n):
+        return (t + (n // 2) * (1 - 2 * t)) * 2 + n % 2
+
+    def kv_z(pc, d):
+        h = lax.rem(a + d, ways)
+        return remote(kvs.at[pc, h], kvbuf.at[s, pc], kv_send.at[pc, d - 1], kv_recv.at[s, pc], h * group + g, t)
+
+    def q_z(pc, d):
+        h = lax.rem(a + d, ways)
+        return remote(qs.at[pc, h], qbuf.at[a, pc], q_send.at[pc, d], q_recv.at[a, pc], h * group + turn(a), t)
+
+    def kv_wait(slot, pc):
+        remote(kvs.at[pc, 0], kvbuf.at[slot, pc], kv_send.at[0, 0], kv_recv.at[slot, pc], s, other).wait_recv()
+
+    def to_across(src, slot, pc, d):
+        return remote(src, kvbuf.at[slot, pc], y_send.at[d, pc], kv_recv.at[slot, pc], across, t)
+
+    def to_mate(src, slot, pc, d):
+        return remote(src, kvbuf.at[slot, pc], m_send.at[d, pc], kv_recv.at[slot, pc], mate, t)
+
+    def prepared(x, scale, pc):
+        outs = []
+        for m in range(2):
+            f = x[m * hd:m * hd + half]
+            b = x[m * hd + half:(m + 1) * hd]
+            mean = (jnp.sum(f * f, axis=0, keepdims=True) + jnp.sum(b * b, axis=0, keepdims=True)) / hd
+            r = lax.rsqrt(mean + 1e-06) * scale
+            f = f * r
+            b = b * r
+            outs.append(f * tab[pc, m, 0] - b * tab[pc, m, 1])
+            outs.append(b * tab[pc, m, 2] + f * tab[pc, m, 3])
+        return jnp.concatenate(outs, axis=0)
+
+    def relay_z(n):
+        pc = piece_of(n)
+        for d in range(1, ways):
+            slot = lax.rem(a + ways - d, ways) * group + g
+            kv_wait(slot, pc)
+            to_across(kvbuf.at[slot, pc], slot, pc, d).start()
+            to_mate(kvbuf.at[slot, pc], slot, pc, d).start()
+
+    def relay_y(n):
+        pc = piece_of(n)
+        for d in range(ways):
+            slot = lax.rem(a + ways - d, ways) * group + (g + 2) % group
+            kv_wait(slot, pc)
+            to_mate(kvbuf.at[slot, pc], slot, pc, ways + d).start()
+
+    for c in loads:
+        c.wait()
+
+    def front(n, carry):
+        pc = piece_of(n)
+
+        @pl.when(n >= 2)
+        def _():
+            tok_copy(n - 2).wait_recv()
+
+        x = toks[n].astype(jnp.float32)
+        x = x * lax.rsqrt(jnp.mean(x * x, axis=-1, keepdims=True) + 1e-06) * gain_ref[...]
+        nrm[...] = x.astype(jnp.bfloat16)
+
+        def product(k, c):
+            raw[k] = jnp.dot(nrm[...], w[k], preferred_element_type=jnp.float32)
+            return c
+
+        lax.fori_loop(0, 5, product, 0)
+
+        def rounded(k, h):
+            return raw[k, :, h * 2 * hd:(h + 1) * 2 * hd].astype(jnp.bfloat16).astype(jnp.float32)
+
+        for h in range(ways):
+            qs[pc, h] = prepared(rounded(0, h).T, hd ** -0.5, pc).astype(jnp.bfloat16)
+            kvs[pc, h, :prow] = prepared(rounded(1, h).T, 1.0, pc).T.astype(jnp.bfloat16)
+            kvs[pc, h, prow:] = raw[2, :, h * vdim:(h + 1) * vdim].astype(jnp.bfloat16).astype(jnp.float32).T.astype(
+                jnp.bfloat16)
+        for d in range(1, ways):
+            kv_z(pc, d).start()
+        to_across(kvs.at[pc, a], s, pc, 0).start()
+        to_mate(kvs.at[pc, a], s, pc, 0).start()
+        for d in range(1, ways):
+            q_z(pc, d).start()
+
+        @pl.when(stays)
+        def _():
+            qbuf[a, pc] = qs[pc, a]
+
+        @pl.when(jnp.logical_not(stays))
+        def _():
+            q_z(pc, 0).start()
+
+        kvbuf[s, pc] = kvs[pc, a]
+        ga = raw[3].astype(jnp.bfloat16).astype(jnp.float32)
+        gg = raw[4].astype(jnp.bfloat16).astype(jnp.float32)
+        gated = (ga * jax.nn.sigmoid(gg)).astype(jnp.bfloat16)
+        gext[pl.ds(pl.multiple_of(32 + pc * prow, 32), prow)] = gated.astype(jnp.float32)
+
+        @pl.when(pc == PIECES - 1)
+        def _():
+            glast[...] = gated[prow - 32:]
+
+        @pl.when(n >= 1)
+        def _():
+            relay_z(n - 1)
+
+        @pl.when(n >= 2)
+        def _():
+            relay_y(n - 2)
+
+        return carry
+
+    halo_out = remote(glast, halo, halo_send.at[0], halo_recv.at[0], lax.rem(s + 1, sp), t)
+    lax.fori_loop(0, PIECES, front, 0)
+
+    @pl.when(s < sp - 1)
+    def _():
+        halo_out.start()
+
+    @pl.when(s > 0)
+    def _():
+        halo_out.wait_recv()
+        gext[0:32] = halo[...].astype(jnp.float32)
+
+    @pl.when(s == 0)
+    def _():
+        gext[0:32] = jnp.zeros((32, cch), jnp.float32)
+
+    def st_copy(r):
+        return remote(st.at[r], str_.at[r], st_send.at[r], st_recv.at[r], s, other)
+
+    def convolve(r, carry):
+        plain = jnp.zeros((prow, 128), jnp.float32)
+        square = jnp.zeros((prow, 128), jnp.float32)
+        for c in range(cch // 128):
+            lanes = slice(c * 128, (c + 1) * 128)
+            window = gext[pl.ds(pl.multiple_of(r * prow, prow), prow + 32), lanes]
+            total = jnp.zeros((prow, 128), jnp.float32)
+            for k in range(8):
+                turned = window if k == 0 else pltpu.roll(window, prow + 32 - k, 0)
+                for j in range(taps):
+                    place = 32 - (taps - 1) + j
+                    if place % 8 == k:
+                        total = total + taps_ref[j:j + 1, lanes] * turned[place - k:place - k + prow]
+            conv[r, :, lanes] = total
+            plain = plain + total
+            square = square + total * total
+        st[r, 0:1] = jnp.sum(plain.T, axis=0, keepdims=True)
+        st[r, 1:2] = jnp.sum(square.T, axis=0, keepdims=True)
+        st_copy(r).start()
+        return carry
+
+    lax.fori_loop(0, PIECES, convolve, 0)
+    relay_z(PIECES - 1)
+
+    def cv_copy(j):
+        return remote(cvo.at[other * 2 + j], cvr.at[j], cv_send.at[j], cv_recv.at[j], s, other)
+
+    def normalize(r, carry):
+        st_copy(r).wait_recv()
+        both = st[r] + str_[r]
+        mean = both[0:1] / channels
+        scale = lax.rsqrt(both[1:2] / channels - mean * mean + 1e-05)
+        mean = jnp.broadcast_to(mean, (128, prow)).T
+        scale = jnp.broadcast_to(scale, (128, prow)).T
+        for c in range(cch // 128):
+            lanes = slice(c * 128, (c + 1) * 128)
+            y = (conv[r, :, lanes] - mean) * scale * cgain_ref[:, lanes] + cshift_ref[:, lanes]
+            cvo[r, :, lanes] = (y * jax.nn.sigmoid(y)).astype(jnp.bfloat16)
+        return carry
+
+    lax.fori_loop(0, PIECES, normalize, 0)
+    for j in range(2):
+        cv_copy(j).start()
+    relay_y(PIECES - 2)
+    relay_y(PIECES - 1)
+    out_load.wait()
+    for j in range(2):
+        cv_copy(j).wait_recv()
+    own = 2 * prow
+    wide = wo.shape[1]
+    step = wide // 4
+    top = ways * tp * vdim
+
+    def conv_part(n, carry):
+        cols = pl.ds(pl.multiple_of(n * step, step), step)
+        mine = wo[pl.ds(pl.multiple_of(top + t * cch, cch), cch), cols]
+        theirs = wo[pl.ds(pl.multiple_of(top + other * cch, cch), cch), cols]
+        macc[:, cols] = jnp.dot(
+            cvo[pl.ds(t * 2, 2)].reshape(own, cch), mine, preferred_element_type=jnp.float32) + jnp.dot(
+            cvr[...].reshape(own, cch), theirs, preferred_element_type=jnp.float32)
+        return carry
+
+    lax.fori_loop(0, 4, conv_part, 0)
+
+    def mate_wait(pc, carry):
+        for b in range(ways):
+            for e in range(2):
+                slot = b * group + (mate - a * group + 2 * e) % group
+                kv_wait(slot, pc)
+        return carry
+
+    lax.fori_loop(0, PIECES, mate_wait, 0)
+
+    def q_wait(i, pc):
+        remote(qs.at[pc, 0], qbuf.at[i, pc], q_send.at[0, 0], q_recv.at[i, pc], s, other).wait_recv()
+
+    def q_waits(i, carry):
+        here = jnp.logical_and(i == a, stays)
+
+        @pl.when(jnp.logical_not(here))
+        def _():
+            for pc in range(PIECES):
+                q_wait(i, pc)
+
+        return carry
+
+    lax.fori_loop(0, ways, q_waits, 0)
+
+    lam = lam_ref[a]
+    head = t * ways + a
+
+    def ao_copy(i, hf, slot):
+        return remote(aos.at[i, hf], ao.at[slot], ao_send.at[i, hf], ao_recv.at[slot], i * group + turn(i), hf)
+
+    def lt_copy(i, slot):
+        return remote(lts.at[i], lor.at[slot], lt_send.at[i], lt_recv.at[slot], i * group + turn(i), t)
+
+    def attend(n, carry):
+        i = lax.rem(a + 1 + n, ways)
+        chunk = i * group + turn(i)
+        queries = [
+            jnp.concatenate([qbuf[i, pc, m * hd:(m + 1) * hd, :] for pc in range(PIECES)], axis=1) for m in range(2)]
+
+        def score(j, ref):
+            for m in range(2):
+                keys = kvbuf[j, :, :prow, m * hd:(m + 1) * hd].reshape(rows, hd)
+                ref[m] = jnp.dot(keys, queries[m], preferred_element_type=jnp.float32)
+
+        def absorb(j, ref, tops, masked=False):
+            vb = jnp.concatenate([kvbuf[j, pc, prow:] for pc in range(PIECES)], axis=1)
+            vb = jnp.concatenate([vb, jnp.ones((16, rows), jnp.bfloat16)], axis=0)
+            out = []
+            for m in range(2):
+                sc = ref[m]
+                if masked:
+                    kp = lax.broadcasted_iota(jnp.int32, sc.shape, 0)
+                    qp = lax.broadcasted_iota(jnp.int32, sc.shape, 1)
+                    sc = jnp.where(kp <= qp, sc, NEG)
+                new = jnp.maximum(tops[m], jnp.max(sc, axis=0, keepdims=True))
+                p = jnp.exp(sc - new)
+                f = jnp.exp(tops[m] - new)
+                acc[m] = acc[m] * f + jnp.dot(vb, p.astype(jnp.bfloat16), preferred_element_type=jnp.float32)
+                out.append(new)
+            return tuple(out)
+
+        acc[...] = jnp.zeros_like(acc)
+        one = jnp.full((1, rows), NEG, jnp.float32)
+        score(chunk, sa)
+        score(0, sb)
+        tops = absorb(chunk, sa, (one, one), True)
+
+        def pair(j, tops):
+            score(2 * j + 1, sa)
+            tops = absorb(2 * j, sb, tops)
+            score(2 * j + 2, sb)
+            return absorb(2 * j + 1, sa, tops)
+
+        tops = lax.fori_loop(0, chunk // 2, pair, tops)
+        tops = lax.cond(chunk % 2 == 1, lambda v: absorb(chunk - 1, sb, v), lambda v: v, tops)
+        l0 = acc[0, vdim:vdim + 1]
+        l1 = acc[1, vdim:vdim + 1]
+        heads = acc[0, :vdim] / l0 - lam * acc[1, :vdim] / l1
+        heads = heads * lax.rsqrt(jnp.mean(heads * heads, axis=0, keepdims=True) + 1e-06)
+        heads = (heads.T * hgain_ref[...]).astype(jnp.bfloat16)
+        lts[i, 0:1] = tops[0] + jnp.log(l0)
+        lts[i, 1:2] = tops[1] + jnp.log(l1)
+        here = jnp.logical_and(i == a, stays)
+        for hf in range(2):
+            aos[i, hf] = heads[hf * own:(hf + 1) * own]
+            mine = jnp.logical_and(here, t == hf)
+
+            @pl.when(mine)
+            def _():
+                ao[head] = heads[hf * own:(hf + 1) * own]
+
+            @pl.when(jnp.logical_not(mine))
+            def _():
+                ao_copy(i, hf, head).start()
+
+        @pl.when(here)
+        def _():
+            lor[a] = lts[i]
+
+        @pl.when(jnp.logical_not(here))
+        def _():
+            lt_copy(i, a).start()
+
+        return carry
+
+    lax.fori_loop(0, ways, attend, 0)
+
+    def gather(h, carry):
+        b = h % ways
+        local = jnp.logical_and(jnp.logical_and(b == a, h // ways == t), stays)
+
+        @pl.when(jnp.logical_not(local))
+        def _():
+            remote(aos.at[0, 0], ao.at[h], ao_send.at[0, 0], ao_recv.at[h], s, other).wait_recv()
+
+        return carry
+
+    lax.fori_loop(0, ways * tp, gather, 0)
+
+    def att_part(n, carry):
+        cols = pl.ds(pl.multiple_of(n * step, step), step)
+        left = jnp.concatenate([ao[h] for h in range(ways * tp)], axis=1)
+        mixed_ref[:, cols] = (
+            macc[:, cols] + jnp.dot(left, wo[:top, cols], preferred_element_type=jnp.float32)).astype(jnp.bfloat16)
+        return carry
+
+    lax.fori_loop(0, 4, att_part, 0)
+
+    for b in range(ways):
+        local = jnp.logical_and(b == a, stays)
+
+        @pl.when(jnp.logical_not(local))
+        def _():
+            remote(lts.at[0], lor.at[b], lt_send.at[0], lt_recv.at[b], s, other).wait_recv()
+
+        for m in range(2):
+            lo_ref[m, b:b + 1] = lor[b, m:m + 1]
+
+    for j in range(2):
+        tok_copy(j).wait_send()
+        cv_copy(j).wait_send()
+
+    def drain(pc, carry):
+        for d in range(1, ways):
+            kv_z(pc, d).wait_send()
+            q_z(pc, d).wait_send()
+
+        @pl.when(jnp.logical_not(stays))
+        def _():
+            q_z(pc, 0).wait_send()
+
+        for d in range(ways):
+            to_across(kvs.at[pc, 0], s, pc, d).wait_send()
+        for d in range(2 * ways):
+            to_mate(kvs.at[pc, 0], s, pc, d).wait_send()
+        st_copy(pc).wait_send()
+        return carry
+
+    lax.fori_loop(0, PIECES, drain, 0)
+
+    @pl.when(s < sp - 1)
+    def _():
+        halo_out.wait_send()
+
+    def drain_out(i, carry):
+        here = jnp.logical_and(i == a, stays)
+        for hf in range(2):
+            @pl.when(jnp.logical_not(jnp.logical_and(here, t == hf)))
+            def _():
+                ao_copy(i, hf, head).wait_send()
+
+        @pl.when(jnp.logical_not(here))
+        def _():
+            lt_copy(i, a).wait_send()
+
+        return carry
+
+    lax.fori_loop(0, ways, drain_out, 0)
+
+
+def whole_layer(
+    sp, tp, tokens, norm_gain, query_weight, key_weight, value_weight, glu_value_weight, glu_gate_weight,
+    qk_gain, mix_lambda, head_gain, conv_kernel, channel_gain, channel_shift, output_weight,
+):
+    ways = mix_lambda.shape[0]
+    group = sp // ways
+    own, width = tokens.shape
+    rows = own * tp
+    prow = rows // PIECES
+    hd = qk_gain.shape[1]
+    half = hd // 2
+    vdim = head_gain.shape[0]
+    taps, cch = conv_kernel.shape
+    me = lax.axis_index("sp")
+    order = jnp.arange(rows, dtype=jnp.int32).reshape(PIECES, 1, prow)
+    positions = (me * rows + order).astype(jnp.float32)
+    inverse = 10000.0 ** (-jnp.arange(0, half, dtype=jnp.float32) * 2.0 / hd)
+    angles = positions * inverse[None, :, None]
+    cosine, sine = jnp.cos(angles)[:, None], jnp.sin(angles)[:, None]
+    first, second = qk_gain[None, :, :half, None], qk_gain[None, :, half:, None]
+    tab = jnp.stack([first * cosine, second * sine, second * cosine, first * sine], axis=2)
+    f32, bf16 = jnp.float32, jnp.bfloat16
+    any_ = pl.BlockSpec(memory_space=pl.ANY)
+    vm = pl.BlockSpec(memory_space=pltpu.VMEM)
+    sm = pl.BlockSpec(memory_space=pltpu.SMEM)
+    dma = pltpu.SemaphoreType.DMA
+    return pl.pallas_call(
+        lambda *refs: layer_kernel((ways, group, tp, taps), *refs),
+        out_shape=(
+            jax.ShapeDtypeStruct((own, output_weight.shape[1]), bf16), jax.ShapeDtypeStruct((2, ways, rows), f32)),
+        in_specs=[any_, vm, any_, any_, any_, any_, any_, any_, sm, vm, vm, vm, vm, any_],
+        out_specs=(vm, vm),
+        scratch_shapes=[
+            pltpu.VMEM((PIECES, prow, width), bf16),
+            pltpu.VMEM((5,) + query_weight.shape, bf16),
+            pltpu.VMEM(tab.shape, f32),
+            pltpu.VMEM(output_weight.shape, bf16),
+            pltpu.VMEM((prow, width), bf16),
+            pltpu.VMEM((5, prow, cch), f32),
+            pltpu.VMEM((PIECES, ways, 2 * hd, prow), bf16),
+            pltpu.VMEM((PIECES, ways, prow + vdim, 2 * hd), bf16),
+            pltpu.VMEM((ways, PIECES, 2 * hd, prow), bf16),
+            pltpu.VMEM((sp, PIECES, prow + vdim, 2 * hd), bf16),
+            pltpu.VMEM((32 + rows, cch), f32),
+            pltpu.VMEM((32, cch), bf16),
+            pltpu.VMEM((32, cch), bf16),
+            pltpu.VMEM((PIECES, prow, cch), f32),
+            pltpu.VMEM((PIECES, prow, cch), bf16),
+            pltpu.VMEM((2, prow, cch), bf16),
+            pltpu.VMEM((PIECES, 2, prow), f32),
+            pltpu.VMEM((PIECES, 2, prow), f32),
+            pltpu.VMEM((own, output_weight.shape[1]), f32),
+            pltpu.VMEM((2, rows, rows), f32),
+            pltpu.VMEM((2, rows, rows), f32),
+            pltpu.VMEM((2, vdim + 16, rows), f32),
+            pltpu.VMEM((ways, 2, own, vdim), bf16),
+            pltpu.VMEM((ways * tp, own, vdim), bf16),
+            pltpu.VMEM((ways, 2, rows), f32),
+            pltpu.VMEM((ways, 2, rows), f32),
+            dma((9,)), dma((2,)), dma((2,)),
+            dma((PIECES, ways)), dma((ways, PIECES)), dma((PIECES, ways - 1)), dma((sp, PIECES)),
+            dma((ways, PIECES)), dma((2 * ways, PIECES)), dma((1,)), dma((1,)),
+            dma((PIECES,)), dma((PIECES,)), dma((2,)), dma((2,)),
+            dma((ways, 2)), dma((ways * tp,)), dma((ways,)), dma((ways,)),
+        ],
+        compiler_params=pltpu.CompilerParams(
+            collective_id=3, has_side_effects=True, vmem_limit_bytes=67043328),
+        name="layer",
+    )(
+        tokens, norm_gain.reshape(1, width), query_weight, key_weight, value_weight, glu_value_weight, glu_gate_weight,
+        tab, mix_lambda, head_gain.reshape(1, vdim), conv_kernel, channel_gain.reshape(1, cch),
+        channel_shift.reshape(1, cch), output_weight)
+
 
 def per_device(
     tokens, norm_gain, query_weight, key_weight, value_weight, glu_value_weight, glu_gate_weight,
@@ -381,6 +892,10 @@
     group = sp // ways
     own = tokens.shape[0]
     rows = own * tp
+    if tp == 2 and ways * group == sp and group == 4 and ways % 2 == 0 and own == 256 and head_size == 64 and value_size == 128:
+        return whole_layer(
+            sp, tp, tokens, norm_gain, query_weight, key_weight, value_weight, glu_value_weight, glu_gate_weight,
+            qk_gain, mix_lambda, head_gain, conv_kernel, channel_gain, channel_shift, output_weight)
 
     def norm(piece):
         inputs = piece.astype(jnp.float32)

time: 172 us -> 94.9 us (0.55)
  waiting for transfers between devices: 18.2 us -> 0 us
  matrix products: 16.4 us -> 0 us
  other arithmetic: 14.3 us -> 1.29 us
  local copies, waits for them, and re-layouts: 15.6 us -> 3.75 us
  Pallas kernels: 96.7 us -> 88 us
  starting transfers between devices: 5.19 us -> 0 us
  blocking collectives: 4.01 us -> 0 us
    ppermute x2 -> x0, waiting for transfers between devices: 18.2 us -> none  [the longest x1 18.2 us: per_device(): lax.ppermute(tokens, 'tp', [(i, (i - d) % tp) for i in range(tp)])]
    dot_general x6 -> x0, matrix products: 16.4 us -> none  [the longest x3 6.93 us: turned(): lax.dot_general(matrix, normed, (((0,), (1,)), ((), ())), preferred_eleme...]
    pallas_call x3 -> x1, Pallas kernels: 96.7 us -> 88 us  [whole_layer(): pl.pallas_call(lambda *refs: layer_kernel((ways, group, tp, taps), *refs)...]
    reduce_sum x2 -> x0, other arithmetic: 5.54 us -> none  [the longest x1 5.05 us: per_device(): jnp.sum(convolved, axis=1)]
    ppermute x2 -> x0, starting transfers between devices: 5.19 us -> none  [the longest x1 4.87 us: from_behind(): lax.ppermute(value, axis, [(source, source + steps) for source in range(l...]
    psum x1 -> x0, blocking collectives: 4.01 us -> none  [per_device(): lax.psum((jnp.sum(convolved, axis=1), jnp.sum(convolved * convolved, axis...]
    concatenate x2 -> x0, other arithmetic: 2.96 us -> none  [the longest x1 2.13 us: per_device(): jnp.concatenate([kk, vt.reshape(heads_here, value_size, rows // 128, 128)...]
    transpose x2 -> x0, local copies, waits for them, and re-layouts: 2.49 us -> none  [the longest x1 1.25 us: per_device(): jnp.transpose(ao, (1, 0, 2)).reshape(own, heads * value_size)]
  transfers between devices with their start and end apart: 2 -> 0, of which waited for: 1 -> 0; matrix products, arithmetic and copies ran while one was open for 13% -> 0% of each run, Pallas kernels for 39% -> 0%
where the time goes in v1:
time: 94.9 us; the launch traced here: 93.7 us
  Pallas kernels  88 us (93%)
  local copies, waits for them, and re-layouts  3.75 us (4%)
  other arithmetic  1.29 us (1%)
    pallas_call x1, Pallas kernels, whole_layer(): pl.pallas_call(lambda *refs: layer_kernel((ways, group, tp, taps), *refs)...  88 us
    unnamed x4, local copies, waits for them, and re-layouts  2.92 us

profile of v1, /device:TPU:11, one launch (start us, length us, event | category | flops | bytes accessed | tf_op | source)
XLA Modules:
  0.0 93.7 jit_solution(10911031908802012613)
XLA Ops:
  0.7 0.8 fusion
  1.5 0.3 multiply_cosine_fusion
  1.8 0.1 broadcast_multiply_fusion.1
  1.9 0.8 pad_maximum_fusion.refs_7_
  2.8 88.0 %layer.1 = (bf16[256,2048]{1,0:T(8,128)(2,1)}, f32[2,4,512]{2,1,0:T(4,128)}) custom-call(bf16[256,2048]{1,0:T(8,128)(2,1)} %refs_0_.1, f32[1,2048]{1,0:T(1,128)} %bitcast.4, bf16[2048,512]{1,0:T(8,128)(2,1)} %refs_2_.1, bf16[2048,512]{1,0:T(8,128)(2,1)} %refs_3_.1, bf16[2048,512]{1,0:T(8,128)(2,1)} %refs_4_.1, bf16[2048,512]{1,0:T(8,128)(2,1)} %refs_5_.1, ...), custom_call_target="tpu_custom_call" | custom-call | tf_op jit(solution)/shard_map/layer/pallas_call | solution.py:829
  90.8 0.0 copy-start
  90.8 2.3 %copy.18 = bf16[256,2048]{1,0:T(8,128)(2,1)} copy(bf16[256,2048]{1,0:T(8,128)(2,1)} %get-tuple-element.14) | data formatting | bytes 2097152
  93.1 0.0 copy-done
  93.1 0.6 copy.19
  (2 shorter events, 0.0 us)
Async XLA Ops:
  90.8 2.3 %copy-start = (f32[2,4,512]{2,1,0:T(4,128)S(1)}, f32[2,4,512]{2,1,0:T(4,128)}, u32[]{:S(2)}) copy-start(f32[2,4,512]{2,1,0:T(4,128)} %get-tuple-element.15) | copy-start | bytes 49156

commit v2 on v1

--- a/solution.py
+++ b/solution.py
@@ -365,11 +365,18 @@
 PIECES = 4
 
 
+def balanced(ways, group):
+    counts = {
+        sum((i * group + (g if i % 2 == 0 else group - 1 - g)) // 2 for i in range(ways)) for g in range(group)}
+    return counts.pop() if len(counts) == 1 else 1
+
+
 def layer_kernel(
-    sizes, tokens_ref, gain_ref, wq_ref, wk_ref, wv_ref, wa_ref, wg_ref, tab_ref, lam_ref, hgain_ref, taps_ref,
-    cgain_ref, cshift_ref, wo_ref, mixed_ref, lo_ref,
+    sizes, tokens_ref, gain_in, wq_ref, wk_ref, wv_ref, wa_ref, wg_ref, qkg_in, lam_in, hgain_in, taps_in,
+    cgain_in, cshift_in, wo_ref, mixed_ref, lo_ref,
+    gain_ref, qkg_ref, lam_ref, hgain_ref, taps_ref, cgain_ref, cshift_ref,
     toks, w, tab, wo, nrm, raw, qs, kvs, qbuf, kvbuf, gext, glast, halo, conv, cvo, cvr, st, str_, macc,
-    sa, sb, acc, aos, ao, lts, lor,
+    sa, sb, acc, top_, aos, ao, lts, lor,
     load, tok_send, tok_recv, q_send, q_recv, kv_send, kv_recv, y_send, m_send, halo_send, halo_recv,
     st_send, st_recv, cv_send, cv_recv, ao_send, ao_recv, lt_send, lt_recv,
 ):
@@ -399,14 +406,17 @@
             src_ref=src, dst_ref=dst, send_sem=send, recv_sem=recv,
             device_id={"sp": row, "tp": col}, device_id_type=MESH)
 
-    loads = [pltpu.make_async_copy(tokens_ref.at[pl.ds(j * prow, prow)], toks.at[j], load.at[j]) for j in range(2)]
-    loads += [
+    small = [
+        pltpu.make_async_copy(src, dst, load.at[8 + n]) for n, (src, dst) in enumerate((
+            (qkg_in, qkg_ref), (gain_in, gain_ref), (lam_in, lam_ref),
+            (hgain_in, hgain_ref), (taps_in, taps_ref), (cgain_in, cgain_ref), (cshift_in, cshift_ref)))]
+    tok_loads = [
+        pltpu.make_async_copy(tokens_ref.at[pl.ds(j * prow, prow)], toks.at[j], load.at[j]) for j in range(2)]
+    weight_loads = [
         pltpu.make_async_copy(ref, w.at[n], load.at[2 + n]) for n, ref in enumerate((wq_ref, wk_ref, wv_ref, wa_ref, wg_ref))]
-    loads.append(pltpu.make_async_copy(tab_ref, tab, load.at[7]))
-    out_load = pltpu.make_async_copy(wo_ref, wo, load.at[8])
-    for c in loads:
+    out_load = pltpu.make_async_copy(wo_ref, wo, load.at[7])
+    for c in small[:2] + tok_loads[:1] + weight_loads[:3] + tok_loads[1:] + weight_loads[3:] + small[2:]:
         c.start()
-    out_load.start()
 
     barrier = pltpu.get_barrier_semaphore()
     flat = s * tp + t
@@ -417,14 +427,33 @@
         return carry
 
     lax.fori_loop(1, sp * tp, greet, 0)
-    pl.semaphore_wait(barrier, sp * tp - 1)
+    small[0].wait()
+    which = lax.broadcasted_iota(jnp.int32, (half, prow), 0)
+    inverse = jnp.zeros((half, prow), jnp.float32)
+    for n in range(half):
+        inverse = jnp.where(which == n, 10000.0 ** (-2.0 * n / hd), inverse)
+    gains = [jnp.broadcast_to(qkg_ref[m:m + 1], (128, hd)).T for m in range(2)]
+
+    def tables(pc, carry):
+        place = s * rows + pc * prow + lax.broadcasted_iota(jnp.int32, (half, prow), 1)
+        angles = place.astype(jnp.float32) * inverse
+        cosine, sine = jnp.cos(angles), jnp.sin(angles)
+        for m in range(2):
+            tab[pc, m, 0] = gains[m][:half] * cosine
+            tab[pc, m, 1] = gains[m][half:] * sine
+            tab[pc, m, 2] = gains[m][half:] * cosine
+            tab[pc, m, 3] = gains[m][:half] * sine
+        return carry
 
     def tok_copy(j):
         return remote(
             tokens_ref.at[pl.ds(j * prow, prow)], toks.at[2 + j], tok_send.at[j], tok_recv.at[j], s, other)
 
-    for j in range(2):
-        tok_copy(j).start()
+    lax.fori_loop(0, PIECES, tables, 0)
+    for n in range(ways):
+        acc[n] = jnp.zeros_like(acc[n])
+        top_[n] = jnp.full_like(top_[n], NEG)
+    small[1].wait()
 
     def piece_of(n):
         return (t + (n // 2) * (1 - 2 * t)) * 2 + n % 2
@@ -474,25 +503,21 @@
             kv_wait(slot, pc)
             to_mate(kvbuf.at[slot, pc], slot, pc, ways + d).start()
 
-    for c in loads:
-        c.wait()
-
-    def front(n, carry):
+    def product(k, n):
+        for j in range(5):
+            @pl.when(jnp.logical_and(n == 0, k == j))
+            def _():
+                weight_loads[j].wait()
+
+        raw[k] = jnp.dot(nrm[...], w[k], preferred_element_type=jnp.float32)
+        return n
+
+    def project(n):
         pc = piece_of(n)
-
-        @pl.when(n >= 2)
-        def _():
-            tok_copy(n - 2).wait_recv()
-
         x = toks[n].astype(jnp.float32)
         x = x * lax.rsqrt(jnp.mean(x * x, axis=-1, keepdims=True) + 1e-06) * gain_ref[...]
         nrm[...] = x.astype(jnp.bfloat16)
-
-        def product(k, c):
-            raw[k] = jnp.dot(nrm[...], w[k], preferred_element_type=jnp.float32)
-            return c
-
-        lax.fori_loop(0, 5, product, 0)
+        lax.fori_loop(0, 3, product, n)
 
         def rounded(k, h):
             return raw[k, :, h * 2 * hd:(h + 1) * 2 * hd].astype(jnp.bfloat16).astype(jnp.float32)
@@ -500,24 +525,61 @@
         for h in range(ways):
             qs[pc, h] = prepared(rounded(0, h).T, hd ** -0.5, pc).astype(jnp.bfloat16)
             kvs[pc, h, :prow] = prepared(rounded(1, h).T, 1.0, pc).T.astype(jnp.bfloat16)
-            kvs[pc, h, prow:] = raw[2, :, h * vdim:(h + 1) * vdim].astype(jnp.bfloat16).astype(jnp.float32).T.astype(
-                jnp.bfloat16)
+            kvs[pc, h, prow:] = rounded(2, h).T.astype(jnp.bfloat16)
+
+    tok_loads[0].wait()
+    project(0)
+    pl.semaphore_wait(barrier, sp * tp - 1)
+    for j in range(2):
+        tok_copy(j).start()
+
+    def front(n, carry):
+        pc = piece_of(n)
+
+        @pl.when(n == 1)
+        def _():
+            tok_loads[1].wait()
+
+        @pl.when(n >= 2)
+        def _():
+            tok_copy(n - 2).wait_recv()
+
+        @pl.when(n >= 1)
+        def _():
+            project(n)
+
+        def send_queries():
+            for d in range(1, ways):
+                q_z(pc, d).start()
+
+            @pl.when(jnp.logical_not(stays))
+            def _():
+                q_z(pc, 0).start()
+
+        @pl.when(n >= 2)
+        def _():
+            send_queries()
+
         for d in range(1, ways):
             kv_z(pc, d).start()
         to_across(kvs.at[pc, a], s, pc, 0).start()
         to_mate(kvs.at[pc, a], s, pc, 0).start()
-        for d in range(1, ways):
-            q_z(pc, d).start()
+
+        @pl.when(n < 2)
+        def _():
+            send_queries()
 
         @pl.when(stays)
         def _():
             qbuf[a, pc] = qs[pc, a]
 
-        @pl.when(jnp.logical_not(stays))
-        def _():
-            q_z(pc, 0).start()
-
         kvbuf[s, pc] = kvs[pc, a]
+
+        @pl.when(n == 1)
+        def _():
+            out_load.start()
+
+        lax.fori_loop(3, 5, product, n)
         ga = raw[3].astype(jnp.bfloat16).astype(jnp.float32)
         gg = raw[4].astype(jnp.bfloat16).astype(jnp.float32)
         gated = (ga * jax.nn.sigmoid(gg)).astype(jnp.bfloat16)
@@ -540,18 +602,22 @@
     halo_out = remote(glast, halo, halo_send.at[0], halo_recv.at[0], lax.rem(s + 1, sp), t)
     lax.fori_loop(0, PIECES, front, 0)
 
+    for c in small[2:]:
+        c.wait()
+
     @pl.when(s < sp - 1)
     def _():
         halo_out.start()
 
-    @pl.when(s > 0)
-    def _():
-        halo_out.wait_recv()
-        gext[0:32] = halo[...].astype(jnp.float32)
-
-    @pl.when(s == 0)
-    def _():
-        gext[0:32] = jnp.zeros((32, cch), jnp.float32)
+    def take_halo():
+        @pl.when(s > 0)
+        def _():
+            halo_out.wait_recv()
+            gext[0:32] = halo[...].astype(jnp.float32)
+
+        @pl.when(s == 0)
+        def _():
+            gext[0:32] = jnp.zeros((32, cch), jnp.float32)
 
     def st_copy(r):
         return remote(st.at[r], str_.at[r], st_send.at[r], st_recv.at[r], s, other)
@@ -577,8 +643,7 @@
         st_copy(r).start()
         return carry
 
-    lax.fori_loop(0, PIECES, convolve, 0)
-    relay_z(PIECES - 1)
+    lax.fori_loop(1, PIECES, convolve, 0)
 
     def cv_copy(j):
         return remote(cvo.at[other * 2 + j], cvr.at[j], cv_send.at[j], cv_recv.at[j], s, other)
@@ -596,14 +661,6 @@
             cvo[r, :, lanes] = (y * jax.nn.sigmoid(y)).astype(jnp.bfloat16)
         return carry
 
-    lax.fori_loop(0, PIECES, normalize, 0)
-    for j in range(2):
-        cv_copy(j).start()
-    relay_y(PIECES - 2)
-    relay_y(PIECES - 1)
-    out_load.wait()
-    for j in range(2):
-        cv_copy(j).wait_recv()
     own = 2 * prow
     wide = wo.shape[1]
     step = wide // 4
@@ -618,17 +675,14 @@
             cvr[...].reshape(own, cch), theirs, preferred_element_type=jnp.float32)
         return carry
 
-    lax.fori_loop(0, 4, conv_part, 0)
-
-    def mate_wait(pc, carry):
+    def mate_wait(n, carry):
+        pc = piece_of(n)
         for b in range(ways):
             for e in range(2):
                 slot = b * group + (mate - a * group + 2 * e) % group
                 kv_wait(slot, pc)
         return carry
 
-    lax.fori_loop(0, PIECES, mate_wait, 0)
-
     def q_wait(i, pc):
         remote(qs.at[pc, 0], qbuf.at[i, pc], q_send.at[0, 0], q_recv.at[i, pc], s, other).wait_recv()
 
@@ -642,10 +696,13 @@
 
         return carry
 
+    lax.fori_loop(0, 2, mate_wait, 0)
     lax.fori_loop(0, ways, q_waits, 0)
 
-    lam = lam_ref[a]
+    lam = jnp.sum(
+        jnp.where(lax.broadcasted_iota(jnp.int32, lam_ref.shape, 1) == a, lam_ref[...], 0.0), axis=1, keepdims=True)
     head = t * ways + a
+    span = 2 * prow
 
     def ao_copy(i, hf, slot):
         return remote(aos.at[i, hf], ao.at[slot], ao_send.at[i, hf], ao_recv.at[slot], i * group + turn(i), hf)
@@ -653,55 +710,142 @@
     def lt_copy(i, slot):
         return remote(lts.at[i], lor.at[slot], lt_send.at[i], lt_recv.at[slot], i * group + turn(i), t)
 
-    def attend(n, carry):
-        i = lax.rem(a + 1 + n, ways)
+    upper = a // (ways // 2)
+    visits = []
+    for k in range(ways - 1):
+        n = k * upper + (ways - 2 - k) * (1 - upper)
+        visits.append(jnp.where(n >= a, n + 1, n))
+    visits.append(a)
+    wide_edges = []
+    edges = []
+    for i in visits:
+        wide_edges.append((wide_edges[-1] if wide_edges else 0) + (i * group + turn(i)) // 2)
+        edges.append((edges[-1] if edges else 0) + i + 1)
+    wide_items = balanced(ways, group) + ways
+    steps = ways * (ways - 1) // 2 + ways
+    wide_steps = wide_items // 2
+
+    def item(x):
+        x = jnp.minimum(x, wide_items + 2 * steps - 1)
+        narrow = jnp.where(x >= wide_items, 1, 0)
+        d = (x - wide_items) // 2
+        last = narrow * (x % 2)
+        q = jnp.where(narrow == 1, d, x - ways)
+        k = 0
+        base = 0
+        for n in range(ways - 1):
+            edge = jnp.where(narrow == 1, edges[n], wide_edges[n])
+            k = jnp.where(q >= edge, n + 1, k)
+            base = jnp.where(q >= edge, edge, base)
+        k = jnp.where(q < 0, x, k)
+        i = visits[-1]
+        for n in range(ways - 1):
+            i = jnp.where(k == n, visits[n], i)
         chunk = i * group + turn(i)
-        queries = [
-            jnp.concatenate([qbuf[i, pc, m * hd:(m + 1) * hd, :] for pc in range(PIECES)], axis=1) for m in range(2)]
-
-        def score(j, ref):
-            for m in range(2):
-                keys = kvbuf[j, :, :prow, m * hd:(m + 1) * hd].reshape(rows, hd)
-                ref[m] = jnp.dot(keys, queries[m], preferred_element_type=jnp.float32)
-
-        def absorb(j, ref, tops, masked=False):
-            vb = jnp.concatenate([kvbuf[j, pc, prow:] for pc in range(PIECES)], axis=1)
-            vb = jnp.concatenate([vb, jnp.ones((16, rows), jnp.bfloat16)], axis=0)
-            out = []
-            for m in range(2):
-                sc = ref[m]
-                if masked:
-                    kp = lax.broadcasted_iota(jnp.int32, sc.shape, 0)
-                    qp = lax.broadcasted_iota(jnp.int32, sc.shape, 1)
-                    sc = jnp.where(kp <= qp, sc, NEG)
-                new = jnp.maximum(tops[m], jnp.max(sc, axis=0, keepdims=True))
-                p = jnp.exp(sc - new)
-                f = jnp.exp(tops[m] - new)
-                acc[m] = acc[m] * f + jnp.dot(vb, p.astype(jnp.bfloat16), preferred_element_type=jnp.float32)
-                out.append(new)
-            return tuple(out)
-
-        acc[...] = jnp.zeros_like(acc)
-        one = jnp.full((1, rows), NEG, jnp.float32)
-        score(chunk, sa)
-        score(0, sb)
-        tops = absorb(chunk, sa, (one, one), True)
-
-        def pair(j, tops):
-            score(2 * j + 1, sa)
-            tops = absorb(2 * j, sb, tops)
-            score(2 * j + 2, sb)
-            return absorb(2 * j + 1, sa, tops)
-
-        tops = lax.fori_loop(0, chunk // 2, pair, tops)
-        tops = lax.cond(chunk % 2 == 1, lambda v: absorb(chunk - 1, sb, v), lambda v: v, tops)
-        l0 = acc[0, vdim:vdim + 1]
-        l1 = acc[1, vdim:vdim + 1]
-        heads = acc[0, :vdim] / l0 - lam * acc[1, :vdim] / l1
+        j = jnp.where(narrow == 1, (q - base + i) % (i + 1), jnp.where(q < 0, chunk // 2, q - base))
+        first = piece_of(2 * narrow + last)
+        slots = [(j * (2 + 2 * narrow) + n // 2 + narrow * (n - n // 2), first + (1 - narrow) * (n % 2)) for n in range(4)]
+        return i, chunk, slots
+
+    def score(x, ref):
+        i, _, slots = item(x)
+        for m in range(2):
+            queries = jnp.concatenate([qbuf[i, pc, m * hd:(m + 1) * hd, :] for pc in range(PIECES)], axis=1)
+            keys = jnp.concatenate([kvbuf[p, q, :prow, m * hd:(m + 1) * hd] for p, q in slots], axis=0)
+            ref[m] = jnp.dot(keys, queries, preferred_element_type=jnp.float32)
+
+    def absorb(x, ref, masked):
+        i, chunk, slots = item(x)
+        vb = jnp.concatenate([kvbuf[p, q, prow:] for p, q in slots], axis=1)
+        vb = jnp.concatenate([vb, jnp.ones((16, rows), jnp.bfloat16)], axis=0)
+        for m in range(2):
+            sc = ref[m]
+            if masked:
+                kp = lax.broadcasted_iota(jnp.int32, (prow, rows), 0)
+                qp = lax.broadcasted_iota(jnp.int32, (prow, rows), 1)
+                ahead = qp - kp
+                sc = jnp.concatenate([
+                    jnp.where(ahead >= (p - chunk) * rows + q * prow, sc[n * prow:(n + 1) * prow], NEG)
+                    for n, (p, q) in enumerate(slots)], axis=0)
+            old = top_[i, m:m + 1]
+            new = jnp.maximum(old, jnp.max(sc, axis=0, keepdims=True))
+            p = jnp.exp(sc - new)
+            f = jnp.exp(old - new)
+            acc[i, m] = acc[i, m] * f + jnp.dot(vb, p.astype(jnp.bfloat16), preferred_element_type=jnp.float32)
+            top_[i, m:m + 1] = new
+
+    def double(y, masked):
+        score(2 * y + 1, sb)
+        absorb(2 * y, sa, masked)
+        score(2 * y + 2, sa)
+        absorb(2 * y + 1, sb, masked)
+
+    def attend(y, carry):
+        d = y - wide_steps
+
+        @pl.when(y == wide_steps - 1)
+        def _():
+            lax.fori_loop(2, 3, mate_wait, 0)
+
+        @pl.when(y == wide_steps)
+        def _():
+            lax.fori_loop(3, 4, mate_wait, 0)
+
+        masked = y < ways // 2
+        for edge in edges[:-1]:
+            masked = jnp.logical_or(masked, d == edge)
+        masked = jnp.logical_or(masked, d == 0)
+
+        @pl.when(masked)
+        def _():
+            double(y, True)
+
+        @pl.when(jnp.logical_not(masked))
+        def _():
+            double(y, False)
+
+        @pl.when(d >= 0)
+        def _():
+            for k in range(ways):
+                @pl.when(d == edges[k] - 1)
+                def _():
+                    finish(visits[k])
+
+        @pl.when(d < 0)
+        def _():
+            @pl.when(y == 1)
+            def _():
+                relay_z(3)
+
+            @pl.when(y == 2)
+            def _():
+                take_halo()
+                lax.fori_loop(0, 1, convolve, 0)
+
+            @pl.when(y == 3)
+            def _():
+                relay_y(2)
+
+            @pl.when(y == 6)
+            def _():
+                lax.fori_loop(0, PIECES, normalize, 0)
+                for j in range(2):
+                    cv_copy(j).start()
+
+            @pl.when(y == 7)
+            def _():
+                relay_y(3)
+
+        return carry
+
+    def finish(i):
+        l0 = acc[i, 0, vdim:vdim + 1]
+        l1 = acc[i, 1, vdim:vdim + 1]
+        heads = acc[i, 0, :vdim] / l0 - lam * acc[i, 1, :vdim] / l1
         heads = heads * lax.rsqrt(jnp.mean(heads * heads, axis=0, keepdims=True) + 1e-06)
         heads = (heads.T * hgain_ref[...]).astype(jnp.bfloat16)
-        lts[i, 0:1] = tops[0] + jnp.log(l0)
-        lts[i, 1:2] = tops[1] + jnp.log(l1)
+        lts[i, 0:1] = top_[i, 0:1] + jnp.log(l0)
+        lts[i, 1:2] = top_[i, 1:2] + jnp.log(l1)
         here = jnp.logical_and(i == a, stays)
         for hf in range(2):
             aos[i, hf] = heads[hf * own:(hf + 1) * own]
@@ -723,9 +867,12 @@
         def _():
             lt_copy(i, a).start()
 
-        return carry
-
-    lax.fori_loop(0, ways, attend, 0)
+    score(0, sa)
+    lax.fori_loop(0, wide_steps + steps, attend, 0)
+    out_load.wait()
+    for j in range(2):
+        cv_copy(j).wait_recv()
+    lax.fori_loop(0, 4, conv_part, 0)
 
     def gather(h, carry):
         b = h % ways
@@ -813,29 +960,27 @@
     half = hd // 2
     vdim = head_gain.shape[0]
     taps, cch = conv_kernel.shape
-    me = lax.axis_index("sp")
-    order = jnp.arange(rows, dtype=jnp.int32).reshape(PIECES, 1, prow)
-    positions = (me * rows + order).astype(jnp.float32)
-    inverse = 10000.0 ** (-jnp.arange(0, half, dtype=jnp.float32) * 2.0 / hd)
-    angles = positions * inverse[None, :, None]
-    cosine, sine = jnp.cos(angles)[:, None], jnp.sin(angles)[:, None]
-    first, second = qk_gain[None, :, :half, None], qk_gain[None, :, half:, None]
-    tab = jnp.stack([first * cosine, second * sine, second * cosine, first * sine], axis=2)
     f32, bf16 = jnp.float32, jnp.bfloat16
     any_ = pl.BlockSpec(memory_space=pl.ANY)
     vm = pl.BlockSpec(memory_space=pltpu.VMEM)
-    sm = pl.BlockSpec(memory_space=pltpu.SMEM)
     dma = pltpu.SemaphoreType.DMA
     return pl.pallas_call(
         lambda *refs: layer_kernel((ways, group, tp, taps), *refs),
         out_shape=(
-            jax.ShapeDtypeStruct((own, output_weight.shape[1]), bf16), jax.ShapeDtypeStruct((2, ways, rows), f32)),
-        in_specs=[any_, vm, any_, any_, any_, any_, any_, any_, sm, vm, vm, vm, vm, any_],
+            pltpu.VMEM((own, output_weight.shape[1]), bf16), pltpu.VMEM((2, ways, rows), f32)),
+        in_specs=[any_] * 14,
         out_specs=(vm, vm),
         scratch_shapes=[
+            pltpu.VMEM((1, width), f32),
+            pltpu.VMEM(qk_gain.shape, f32),
+            pltpu.VMEM((1, ways), f32),
+            pltpu.VMEM((1, vdim), f32),
+            pltpu.VMEM((taps, cch), f32),
+            pltpu.VMEM((1, cch), f32),
+            pltpu.VMEM((1, cch), f32),
             pltpu.VMEM((PIECES, prow, width), bf16),
             pltpu.VMEM((5,) + query_weight.shape, bf16),
-            pltpu.VMEM(tab.shape, f32),
+            pltpu.VMEM((PIECES, 2, 4, half, prow), f32),
             pltpu.VMEM(output_weight.shape, bf16),
             pltpu.VMEM((prow, width), bf16),
             pltpu.VMEM((5, prow, cch), f32),
@@ -854,23 +999,24 @@
             pltpu.VMEM((own, output_weight.shape[1]), f32),
             pltpu.VMEM((2, rows, rows), f32),
             pltpu.VMEM((2, rows, rows), f32),
-            pltpu.VMEM((2, vdim + 16, rows), f32),
+            pltpu.VMEM((ways, 2, vdim + 16, rows), f32),
+            pltpu.VMEM((ways, 2, rows), f32),
             pltpu.VMEM((ways, 2, own, vdim), bf16),
             pltpu.VMEM((ways * tp, own, vdim), bf16),
             pltpu.VMEM((ways, 2, rows), f32),
             pltpu.VMEM((ways, 2, rows), f32),
-            dma((9,)), dma((2,)), dma((2,)),
+            dma((16,)), dma((2,)), dma((2,)),
             dma((PIECES, ways)), dma((ways, PIECES)), dma((PIECES, ways - 1)), dma((sp, PIECES)),
             dma((ways, PIECES)), dma((2 * ways, PIECES)), dma((1,)), dma((1,)),
             dma((PIECES,)), dma((PIECES,)), dma((2,)), dma((2,)),
             dma((ways, 2)), dma((ways * tp,)), dma((ways,)), dma((ways,)),
         ],
         compiler_params=pltpu.CompilerParams(
-            collective_id=3, has_side_effects=True, vmem_limit_bytes=67043328),
+            collective_id=3, has_side_effects=True, vmem_limit_bytes=62000000),
         name="layer",
     )(
         tokens, norm_gain.reshape(1, width), query_weight, key_weight, value_weight, glu_value_weight, glu_gate_weight,
-        tab, mix_lambda, head_gain.reshape(1, vdim), conv_kernel, channel_gain.reshape(1, cch),
+        qk_gain, mix_lambda.reshape(1, ways), head_gain.reshape(1, vdim), conv_kernel, channel_gain.reshape(1, cch),
         channel_shift.reshape(1, cch), output_weight)
 
 
@@ -892,7 +1038,7 @@
     group = sp // ways
     own = tokens.shape[0]
     rows = own * tp
-    if tp == 2 and ways * group == sp and group == 4 and ways % 2 == 0 and own == 256 and head_size == 64 and value_size == 128:
+    if tp == 2 and ways * group == sp and group == 4 and balanced(ways, group) % 2 == 0 and ways % 2 == 0 and ways == group and own == 256 and head_size == 64 and value_size == 128:
         return whole_layer(
             sp, tp, tokens, norm_gain, query_weight, key_weight, value_weight, glu_value_weight, glu_gate_weight,
             qk_gain, mix_lambda, head_gain, conv_kernel, channel_gain, channel_shift, output_weight)

time: 94.9 us -> 82.5 us (0.87); the launches traced: 93.7 us -> 82.4 us
  Pallas kernels: 88 us -> 80.2 us
  local copies, waits for them, and re-layouts: 3.75 us -> 1.58 us
  other arithmetic: 1.29 us -> 0 us
    pallas_call x1, Pallas kernels: 88 us -> 80.2 us  [whole_layer(): pl.pallas_call(lambda *refs: layer_kernel((ways, group, tp, taps), *refs)...]
    unnamed x4 -> x2, local copies, waits for them, and re-layouts: 2.92 us -> 1.58 us
where the time goes in v2:
time: 82.5 us; the launch traced here: 82.4 us
  Pallas kernels  80.2 us (97%)
  local copies, waits for them, and re-layouts  1.58 us (2%)
    pallas_call x1, Pallas kernels, whole_layer(): pl.pallas_call(lambda *refs: layer_kernel((ways, group, tp, taps), *refs)...  80.2 us

profile of v2, /device:TPU:11, one launch (start us, length us, event | category | flops | bytes accessed | tf_op | source)
XLA Modules:
  0.0 82.4 jit_solution(8748083337207655180)
XLA Ops:
  0.6 80.2 %layer.1 = (bf16[256,2048]{1,0:T(8,128)(2,1)S(1)}, f32[2,4,512]{2,1,0:T(4,128)S(1)}) custom-call(bf16[256,2048]{1,0:T(8,128)(2,1)} %refs_0_.1, f32[1,2048]{1,0:T(1,128)} %bitcast.5, bf16[2048,512]{1,0:T(8,128)(2,1)} %refs_2_.1, bf16[2048,512]{1,0:T(8,128)(2,1)} %refs_3_.1, bf16[2048,512]{1,0:T(8,128)(2,1)} %refs_4_.1, bf16[2048,512]{1,0:T(8,128)(2,1)} %refs_5_.1, ...), custom_call_target="tpu_custom_call" | custom-call | tf_op jit(solution)/shard_map/layer/pallas_call | solution.py:967
  80.8 1.0 %copy.18 = bf16[256,2048]{1,0:T(8,128)(2,1)} copy(bf16[256,2048]{1,0:T(8,128)(2,1)S(1)} %get-tuple-element.2) | data formatting | bytes 2097152
  81.8 0.6 copy.19

commit v3 on v2

--- a/solution.py
+++ b/solution.py
@@ -523,7 +523,7 @@
             return raw[k, :, h * 2 * hd:(h + 1) * 2 * hd].astype(jnp.bfloat16).astype(jnp.float32)
 
         for h in range(ways):
-            qs[pc, h] = prepared(rounded(0, h).T, hd ** -0.5, pc).astype(jnp.bfloat16)
+            qs[pc, h] = prepared(rounded(0, h).T, hd ** -0.5 / math.log(2.0), pc).astype(jnp.bfloat16)
             kvs[pc, h, :prow] = prepared(rounded(1, h).T, 1.0, pc).T.astype(jnp.bfloat16)
             kvs[pc, h, prow:] = rounded(2, h).T.astype(jnp.bfloat16)
 
@@ -769,8 +769,8 @@
                     for n, (p, q) in enumerate(slots)], axis=0)
             old = top_[i, m:m + 1]
             new = jnp.maximum(old, jnp.max(sc, axis=0, keepdims=True))
-            p = jnp.exp(sc - new)
-            f = jnp.exp(old - new)
+            p = jnp.exp2(sc - new)
+            f = jnp.exp2(old - new)
             acc[i, m] = acc[i, m] * f + jnp.dot(vb, p.astype(jnp.bfloat16), preferred_element_type=jnp.float32)
             top_[i, m:m + 1] = new
 
@@ -780,61 +780,40 @@
         score(2 * y + 2, sa)
         absorb(2 * y + 1, sb, masked)
 
-    def attend(y, carry):
-        d = y - wide_steps
-
-        @pl.when(y == wide_steps - 1)
-        def _():
-            lax.fori_loop(2, 3, mate_wait, 0)
-
-        @pl.when(y == wide_steps)
-        def _():
-            lax.fori_loop(3, 4, mate_wait, 0)
-
-        masked = y < ways // 2
+    def masked_pair(y, carry):
+        double(y, True)
+        return carry
+
+    def plain_pair(y, carry):
+        double(y, False)
+        return carry
+
+    def attend(d, carry):
+        masked = d == 0
         for edge in edges[:-1]:
             masked = jnp.logical_or(masked, d == edge)
-        masked = jnp.logical_or(masked, d == 0)
 
         @pl.when(masked)
         def _():
-            double(y, True)
+            double(d + wide_steps, True)
 
         @pl.when(jnp.logical_not(masked))
         def _():
-            double(y, False)
-
-        @pl.when(d >= 0)
-        def _():
-            for k in range(ways):
-                @pl.when(d == edges[k] - 1)
-                def _():
-                    finish(visits[k])
-
-        @pl.when(d < 0)
-        def _():
-            @pl.when(y == 1)
-            def _():
-                relay_z(3)
-
-            @pl.when(y == 2)
-            def _():
-                take_halo()
-                lax.fori_loop(0, 1, convolve, 0)
-
-            @pl.when(y == 3)
-            def _():
-                relay_y(2)
-
-            @pl.when(y == 6)
-            def _():
-                lax.fori_loop(0, PIECES, normalize, 0)
-                for j in range(2):
-                    cv_copy(j).start()
-
-            @pl.when(y == 7)
-            def _():
-                relay_y(3)
+            double(d + wide_steps, False)
+
+        done = d == edges[-1] - 1
+        for edge in edges[:-1]:
+            done = jnp.logical_or(done, d == edge - 1)
+
+        @pl.when(done)
+        def _():
+            k = 0
+            for n, edge in enumerate(edges[:-1]):
+                k = jnp.where(d >= edge, n + 1, k)
+            i = visits[-1]
+            for n in range(ways - 1):
+                i = jnp.where(k == n, visits[n], i)
+            finish(i)
 
         return carry
 
@@ -844,8 +823,8 @@
         heads = acc[i, 0, :vdim] / l0 - lam * acc[i, 1, :vdim] / l1
         heads = heads * lax.rsqrt(jnp.mean(heads * heads, axis=0, keepdims=True) + 1e-06)
         heads = (heads.T * hgain_ref[...]).astype(jnp.bfloat16)
-        lts[i, 0:1] = top_[i, 0:1] + jnp.log(l0)
-        lts[i, 1:2] = top_[i, 1:2] + jnp.log(l1)
+        lts[i, 0:1] = top_[i, 0:1] * math.log(2.0) + jnp.log(l0)
+        lts[i, 1:2] = top_[i, 1:2] * math.log(2.0) + jnp.log(l1)
         here = jnp.logical_and(i == a, stays)
         for hf in range(2):
             aos[i, hf] = heads[hf * own:(hf + 1) * own]
@@ -868,29 +847,57 @@
             lt_copy(i, a).start()
 
     score(0, sa)
-    lax.fori_loop(0, wide_steps + steps, attend, 0)
+    lax.fori_loop(0, ways // 2, masked_pair, 0)
+    relay_z(3)
+    cuts = (ways // 2, ways // 2 + 2, wide_steps - 2, wide_steps)
+    lax.fori_loop(cuts[0], cuts[1], plain_pair, 0)
+    take_halo()
+    lax.fori_loop(0, 1, convolve, 0)
+    relay_y(2)
+    lax.fori_loop(cuts[1], cuts[2], plain_pair, 0)
+    lax.fori_loop(0, PIECES, normalize, 0)
+    for j in range(2):
+        cv_copy(j).start()
+    relay_y(3)
+    lax.fori_loop(2, 3, mate_wait, 0)
+    lax.fori_loop(cuts[2], cuts[3], plain_pair, 0)
+    lax.fori_loop(3, 4, mate_wait, 0)
+    lax.fori_loop(0, steps, attend, 0)
     out_load.wait()
     for j in range(2):
         cv_copy(j).wait_recv()
     lax.fori_loop(0, 4, conv_part, 0)
 
-    def gather(h, carry):
-        b = h % ways
-        local = jnp.logical_and(jnp.logical_and(b == a, h // ways == t), stays)
-
-        @pl.when(jnp.logical_not(local))
-        def _():
-            remote(aos.at[0, 0], ao.at[h], ao_send.at[0, 0], ao_recv.at[h], s, other).wait_recv()
-
-        return carry
-
-    lax.fori_loop(0, ways * tp, gather, 0)
+    def gather(n):
+        b = lax.rem(a + n, ways)
+        for e in range(tp):
+            local = jnp.logical_and(stays, t == e) if n == 0 else False
+
+            @pl.when(jnp.logical_not(local))
+            def _():
+                remote(
+                    aos.at[0, 0], ao.at[e * ways + b], ao_send.at[0, 0], ao_recv.at[e * ways + b], s, other).wait_recv()
+
+    def product_of(offsets, cols):
+        heads = [e * ways + lax.rem(a + n, ways) for n in offsets for e in range(tp)]
+        left = jnp.concatenate([ao[h] for h in heads], axis=1)
+        right = jnp.concatenate([wo[pl.ds(pl.multiple_of(h * vdim, vdim), vdim), cols] for h in heads], axis=0)
+        return jnp.dot(left, right, preferred_element_type=jnp.float32)
+
+    for n in range(1, ways):
+        gather(n)
+
+    def far_part(n, carry):
+        cols = pl.ds(pl.multiple_of(n * step, step), step)
+        macc[:, cols] += product_of(range(1, ways), cols)
+        return carry
+
+    lax.fori_loop(0, 4, far_part, 0)
+    gather(0)
 
     def att_part(n, carry):
         cols = pl.ds(pl.multiple_of(n * step, step), step)
-        left = jnp.concatenate([ao[h] for h in range(ways * tp)], axis=1)
-        mixed_ref[:, cols] = (
-            macc[:, cols] + jnp.dot(left, wo[:top, cols], preferred_element_type=jnp.float32)).astype(jnp.bfloat16)
+        mixed_ref[:, cols] = (macc[:, cols] + product_of([0], cols)).astype(jnp.bfloat16)
         return carry
 
     lax.fori_loop(0, 4, att_part, 0)

time: 82.5 us -> 78.1 us (0.947)
  Pallas kernels: 80.2 us -> 75.6 us
    pallas_call x1, Pallas kernels: 80.2 us -> 75.6 us  [whole_layer(): pl.pallas_call(lambda *refs: layer_kernel((ways, group, tp, taps), *refs)...]
where the time goes in v3:
time: 78.1 us; the launch traced here: 77.9 us
  Pallas kernels  75.6 us (97%)
  local copies, waits for them, and re-layouts  1.58 us (2%)
    pallas_call x1, Pallas kernels, whole_layer(): pl.pallas_call(lambda *refs: layer_kernel((ways, group, tp, taps), *refs)...  75.6 us
    unnamed x2, local copies, waits for them, and re-layouts  1.58 us

profile of v3, /device:TPU:11, one launch (start us, length us, event | category | flops | bytes accessed | tf_op | source)
XLA Modules:
  0.0 77.9 jit_solution(17051833245024753887)
XLA Ops:
  0.6 75.6 %layer.1 = (bf16[256,2048]{1,0:T(8,128)(2,1)S(1)}, f32[2,4,512]{2,1,0:T(4,128)S(1)}) custom-call(bf16[256,2048]{1,0:T(8,128)(2,1)} %refs_0_.1, f32[1,2048]{1,0:T(1,128)} %bitcast.5, bf16[2048,512]{1,0:T(8,128)(2,1)} %refs_2_.1, bf16[2048,512]{1,0:T(8,128)(2,1)} %refs_3_.1, bf16[2048,512]{1,0:T(8,128)(2,1)} %refs_4_.1, bf16[2048,512]{1,0:T(8,128)(2,1)} %refs_5_.1, ...), custom_call_target="tpu_custom_call" | custom-call | tf_op jit(solution)/shard_map/layer/pallas_call | solution.py:974
  76.3 1.0 %copy.18 = bf16[256,2048]{1,0:T(8,128)(2,1)} copy(bf16[256,2048]{1,0:T(8,128)(2,1)S(1)} %get-tuple-element.2) | data formatting | bytes 2097152
  77.3 0.6 copy.19
